TPU v7x, 256 devices: a whole 4x4x8 slice. The times are simulated.
256 devices in a mesh: sp: 16 (over y, x), tp: 16 (over z, core).
Axes of the slice: x: 4, y: 4, z: 8, core: 2. Of those that a mesh axis runs over, the one named last changes fastest.
Arguments:
- conv_value: bfloat16 [49152, 2048], P('sp', 'tp'), may hold values from -48 to 48
- conv_gate: bfloat16 [49152, 2048], P('sp', 'tp'), may hold values from -6 to 6
- doc_ids: int32 [49152], P('sp'), may hold values from 0 to 15, never falling along the last dimension, each value on 1 to 9216 neighbouring positions
- conv_kernel: bfloat16 [31, 2048], P(None, 'tp'), may hold values from -1 to 1
- norm_gain_conv: float32 [2048], replicated, may hold values from 0.1 to 1.9
- norm_bias_conv: float32 [2048], replicated, may hold values from -3 to 3
- proj_weight: bfloat16 [2048, 2048], P('tp'), may hold values from -0.125 to 0.125
- residual: bfloat16 [49152, 2048], P(('sp', 'tp')), may hold values from -6 to 6
- norm_gain_moe: float32 [2048], replicated, may hold values from 0.1 to 1.9
- group_router: bfloat16 [2048, 2], replicated, may hold values from -0.125 to 0.125
- expert_router: bfloat16 [2048, 16], replicated, may hold values from -0.125 to 0.125
- routing: int32 [49152, 2], P(('sp', 'tp')), may hold values from 0 to 15, as said below
- expert_gate_w: bfloat16 [16, 2048, 512], P('sp'), may hold values from -0.125 to 0.125
- expert_up_w: bfloat16 [16, 2048, 512], P('sp'), may hold values from -0.125 to 0.125
- expert_down_w: bfloat16 [16, 512, 2048], P('sp'), may hold values from -0.25 to 0.25
Outputs:
- output: bfloat16 [49152, 2048], P(('sp', 'tp'))
Inputs may be any that keep to these rules, and one draw needn't show every extreme that they name: `routing`: both numbers of a row are different experts of one group (expert // 8); within the rows of one device (aligned blocks of 192 rows) every expert is named exactly 24 times.
All inputs are finite; a program needn't handle non-finite values.
Results may differ from a plain program's by a relative error of at most 0.015.
Values may be sent and summed in bfloat16 or wider, within the bound.
A program may use at most 64 MiB of HBM per device.

v0:
```python
import jax
import jax.numpy as jnp
from jax import lax
from jax.sharding import PartitionSpec as P

epsilon = 1e-06


def shifted(array, axis, by):
    count = lax.axis_size(axis)
    pairs = [(i, i + by) for i in range(count) if 0 <= i + by < count]
    return lax.ppermute(array, axis, pairs)


def project_rows(activated_rows, proj_weight):
    return jnp.dot(
        activated_rows,
        lax.all_gather(proj_weight, "tp", axis=0, tiled=True),
        preferred_element_type=jnp.float32,
    )


def body(
    conv_value,
    conv_gate,
    doc_ids,
    conv_kernel,
    norm_gain_conv,
    norm_bias_conv,
    proj_weight,
    residual,
    norm_gain_moe,
    group_router,
    expert_router,
    routing,
    expert_gate_w,
    expert_up_w,
    expert_down_w,
):
    local_tokens, local_width = conv_value.shape
    kernel_taps = conv_kernel.shape[0]
    rim_width = kernel_taps - 1
    gated_values = (
        conv_value.astype(jnp.float32) * jax.nn.sigmoid(conv_gate.astype(jnp.float32))
    ).astype(jnp.bfloat16)
    rim_values, rim_ids = shifted(
        (gated_values[local_tokens - rim_width :], doc_ids[local_tokens - rim_width :]), "sp", 1
    )
    padded = jnp.concatenate([rim_values, gated_values], axis=0)
    padded_ids = jnp.concatenate([rim_ids, doc_ids], axis=0)
    kernel = conv_kernel.astype(jnp.float32)
    summed = jnp.zeros((local_tokens, local_width), jnp.float32)
    for tap in range(kernel_taps):
        same_doc = padded_ids[tap : tap + local_tokens] == doc_ids
        summed = summed + jnp.where(
            same_doc[:, None],
            padded[tap : tap + local_tokens].astype(jnp.float32) * kernel[tap][None, :],
            jnp.float32(0.0),
        )
    convolved = summed.astype(jnp.bfloat16)
    raw_rows = lax.all_to_all(convolved, "tp", split_axis=0, concat_axis=1, tiled=True)
    raw_values = raw_rows.astype(jnp.float32)
    average = jnp.mean(raw_values, axis=1, keepdims=True)
    centered = raw_values - average
    variance = jnp.mean(centered * centered, axis=1, keepdims=True)
    moved_rows = jax.nn.silu(
        centered * lax.rsqrt(variance + epsilon) * norm_gain_conv + norm_bias_conv
    ).astype(jnp.bfloat16)
    projected = project_rows(moved_rows, proj_weight)
    state_values = residual.astype(jnp.float32) + projected
    hidden_state = state_values.astype(jnp.bfloat16)
    state_values = hidden_state.astype(jnp.float32)
    normed = (
        state_values
        * lax.rsqrt(jnp.mean(state_values * state_values, axis=1, keepdims=True) + epsilon)
        * norm_gain_moe
    ).astype(jnp.bfloat16)
    group_logits = jnp.dot(normed, group_router, preferred_element_type=jnp.float32)
    expert_logits = jnp.dot(normed, expert_router, preferred_element_type=jnp.float32)
    group_total = group_router.shape[1]
    expert_total = expert_router.shape[1]
    per_group = expert_total // group_total
    first_choice = routing[:, 0]
    second_choice = routing[:, 1]
    chosen_group = first_choice // per_group
    group_exp = jnp.exp(group_logits)
    group_match = chosen_group[:, None] == jnp.arange(group_total, dtype=jnp.int32)[None, :]
    group_prob = jnp.sum(jnp.where(group_match, group_exp, jnp.float32(0.0)), axis=1) / jnp.sum(
        group_exp, axis=1
    )
    expert_iota = jnp.arange(expert_total, dtype=jnp.int32)[None, :]
    first_logit = jnp.sum(
        jnp.where(first_choice[:, None] == expert_iota, expert_logits, jnp.float32(0.0)), axis=1
    )
    second_logit = jnp.sum(
        jnp.where(second_choice[:, None] == expert_iota, expert_logits, jnp.float32(0.0)), axis=1
    )
    first_exp = jnp.exp(first_logit)
    second_exp = jnp.exp(second_logit)
    first_weight = group_prob * first_exp / (first_exp + second_exp)
    second_weight = group_prob * second_exp / (first_exp + second_exp)
    row_count = normed.shape[0]
    capacity = 2 * row_count // expert_total
    flat_experts = routing.reshape(-1)
    indicator = (flat_experts[:, None] == expert_iota).astype(jnp.int32)
    before = jnp.cumsum(indicator, axis=0) - indicator
    position = jnp.sum(before * indicator, axis=1)
    destination = flat_experts * capacity + position
    source = (
        jnp.zeros((2 * row_count,), jnp.int32)
        .at[destination]
        .set(jnp.arange(2 * row_count, dtype=jnp.int32) // 2)
    )
    outgoing = normed[source].reshape(expert_total, capacity, normed.shape[1])
    arrived = lax.all_to_all(outgoing, "sp", split_axis=0, concat_axis=0, tiled=True)
    senders, slot_count, features = arrived.shape
    flattened = arrived.reshape(senders * slot_count, features)
    gate_part = jnp.dot(flattened, expert_gate_w[0], preferred_element_type=jnp.float32)
    up_part = jnp.dot(flattened, expert_up_w[0], preferred_element_type=jnp.float32)
    expert_hidden = (jax.nn.silu(gate_part) * up_part).astype(jnp.bfloat16)
    expert_result = jnp.dot(
        expert_hidden, expert_down_w[0], preferred_element_type=jnp.float32
    ).astype(jnp.bfloat16)
    returned = lax.all_to_all(
        expert_result.reshape(senders, slot_count, features),
        "sp",
        split_axis=0,
        concat_axis=0,
        tiled=True,
    )
    picked = (
        returned.reshape(2 * row_count, normed.shape[1])[destination]
        .reshape(row_count, 2, normed.shape[1])
        .astype(jnp.float32)
    )
    mixture = first_weight[:, None] * picked[:, 0] + second_weight[:, None] * picked[:, 1]
    return (state_values + mixture).astype(jnp.bfloat16)


def solution(mesh):
    placed = (
        P("sp", "tp"),
        P("sp", "tp"),
        P("sp"),
        P(None, "tp"),
        P(),
        P(),
        P("tp", None),
        P(("sp", "tp"), None),
        P(),
        P(),
        P(),
        P(("sp", "tp"), None),
        P("sp", None, None),
        P("sp", None, None),
        P("sp", None, None),
    )
    return jax.shard_map(
        body, mesh=mesh, in_specs=placed, out_specs=P(("sp", "tp"), None), check_vma=False
    )
```

profile of v0, /device:TPU:1, one launch (start us, length us, event | category | flops | bytes accessed | tf_op | source)
XLA Modules:
  0.0 185.8 jit_solution(3365401490658242660)
XLA Ops:
  6.5 0.7 all-gather.2.cloned.1.call-update
  7.3 0.8 slice.297
  8.0 3.9 %collective-permute-start = (s32[30]{0:T(128)S(1)}, s32[30]{0:T(128)S(1)}, u32[]{:S(2)}, u32[]{:S(2)}) collective-permute-start(s32[30]{0:T(128)S(1)} %slice.297), channel_id=1, source_target_pairs={{0,16},{16,32},{32,48},{48,64},{64,80},{80,96},{96,112},{112,128},... | collective-permute-start | bytes 368 | tf_op jit(solution)/shard_map/ppermute | solution.py:12
  12.0 1.8 multiply_convert_fusion.2
  13.8 3.1 %collective-permute-start.1 = (bf16[30,128]{1,0:T(8,128)(2,1)S(1)}, bf16[30,128]{1,0:T(8,128)(2,1)S(1)}, u32[]{:S(2)}, u32[]{:S(2)}) collective-permute-start(bf16[30,128]{1,0:T(8,128)(2,1)S(1)} %slice.402), channel_id=1, source_target_pairs={{0,16},{16,32},{32,48},{48,64},{64,80},{80,96},{96,112},{112,128},... | collective-permute-start | bytes 23048 | tf_op jit(solution)/shard_map/ppermute | solution.py:12
  16.9 0.0 collective-permute-done
  17.0 0.1 fusion.72
  17.1 0.1 fusion.74
  17.2 0.1 fusion.76
  17.3 0.1 fusion.126
  17.4 0.3 collective-permute-done.1
  17.7 16.6 %add_convert_fusion = bf16[3072,128]{1,0:T(8,128)(2,1)} fusion(bf16[3072,128]{1,0:T(8,128)(2,1)S(1)} %multiply_convert_fusion.2, bf16[30,128]{1,0:T(8,128)(2,1)S(1)} %collective-permute-done.1, f32[128]{0:T(128)S(1)} %get-tuple-element.14, f32[128]{0:T(128)S(1)} %get-tuple-element.15, f32[128]{0:T(128)S(1)} %get-tuple-element.16, ...), kind=kLoop, calls=%fused_computation.60 | loop fusion | flops 83755008 | bytes 1688576 | tf_op jit(solution)/shard_map/convert_element_type | solution.py:60
  34.2 10.4 %all-to-all-start = ((bf16[16,192,128]{2,1,0:T(8,128)(2,1)}), bf16[16,192,128]{2,1,0:T(8,128)(2,1)S(1)}, u32[]{:S(2)}, u32[]{:S(2)}) async-start(bf16[16,192,128]{2,1,0:T(8,128)(2,1)} %bitcast.147), calls=%async_computation | async-start | bytes 1572864 | tf_op jit(solution)/shard_map/all_to_all | solution.py:61
  44.7 0.0 copy-done.6
  44.7 0.1 copy.25
  44.8 0.1 eq.206
  44.9 0.1 eq.202
  45.1 0.9 reduce-window.6
  46.0 0.2 slice_reduce_fusion
  46.2 0.1 copy.24
  46.4 0.1 mul.522
  46.5 0.1 fusion.67
  46.6 2.9 %scatter_custom_fusion = s32[384]{0:T(512)S(1)} fusion(s32[384]{0:T(512)S(1)} %fusion.132, s32[384]{0:T(512)S(1)} %add_select_fusion, s32[]{:T(128)} %constant.50.clone.1), kind=kCustom, calls=%fused_computation.261 | custom fusion | bytes 1540 | tf_op jit(solution)/shard_map/scatter | solution.py:112
  49.6 25.1 %all-to-all-done = bf16[16,192,128]{2,1,0:T(8,128)(2,1)S(1)} async-done(((bf16[16,192,128]{2,1,0:T(8,128)(2,1)}), bf16[16,192,128]{2,1,0:T(8,128)(2,1)S(1)}, u32[]{:S(2)}, u32[]{:S(2)}) %all-to-all-start) | async-done | bytes 786464 | tf_op jit(solution)/shard_map/all_to_all | solution.py:61
  74.7 0.2 convert_reduce_fusion
  74.9 0.4 fusion.8
  75.3 0.0 copy-start.7
  75.3 10.8 %all-gather.2.cloned.1.call-done = bf16[2048,2048]{1,0:T(8,128)(2,1)} async-done(((bf16[128,2048]{1,0:T(8,128)(2,1)}), bf16[2048,2048]{1,0:T(8,128)(2,1)}) %all-gather.2.cloned.1.call-update) | async-done | bytes 8388624 | tf_op jit(solution)/shard_map/all_gather | solution.py:18
  86.1 0.0 copy-done.11
  86.1 5.7 %multiply_reduce_fusion = (f32[192]{0:T(256)S(1)}, f32[192,2048]{1,0:T(8,128)S(1)}) fusion(bf16[2048,2048]{1,0:T(8,128)(2,1)} %all-gather.2.cloned.1.call-done, f32[2048]{0:T(1024)S(1)} %copy-done.11, f32[2048]{0:T(1024)S(1)} %copy-done.12, f32[192]{0:T(256)S(1)} %add_rsqrt_fusion.1, f32[192]{0:T(256)S(1)} %broadcast_multiply_fusion.1, ...), kind=kOutput, calls=%fused_computation.58 | convolution fusion | flops 1616903936 | bytes 11553024 | tf_op jit(solution)/shard_map/dot_general | solution.py:16
  91.8 0.0 copy-start.1
  91.8 1.1 copy-done.1
  92.9 0.0 copy-done.7
  92.9 0.2 multiply_convert_fusion
  93.1 3.1 %gather_fusion = bf16[384,2048]{1,0:T(8,128)(2,1)} fusion(bf16[192,2048]{1,0:T(8,128)(2,1)S(1)} %multiply_convert_fusion, s32[1024]{0:T(1024)S(1)} %pad_clamp_fusion.1), kind=kCustom, calls=%fused_computation | custom fusion | bytes 3147264 | tf_op jit(solution)/shard_map/gather | solution.py:114
  96.3 28.7 %all_to_all.23 = bf16[16,24,2048]{2,1,0:T(8,128)(2,1)S(1)} all-to-all(bf16[16,24,2048]{2,1,0:T(8,128)(2,1)} %bitcast.146), channel_id=1, replica_groups=mesh['sp'=16,'tp'=16] {'sp'}, dimensions={0} | all-to-all | bytes 3145728 | tf_op jit(solution)/shard_map/all_to_all | solution.py:115
  125.0 1.2 copy-done.3
  126.2 1.9 fusion.5
  128.0 5.3 %convolution_convert_fusion = bf16[384,2048]{1,0:T(8,128)(2,1)} fusion(bf16[1,512,2048]{2,1,0:T(8,128)(2,1)S(1)} %copy-done, bf16[384,2048]{1,0:T(8,128)(2,1)} %bitcast.150, bf16[1,2048,512]{2,1,0:T(8,128)(2,1)} %param.28, f32[384,512]{1,0:T(8,128)} %fusion.5), kind=kOutput, calls=%fused_computation.32 | convolution fusion | flops 1612578816 | bytes 8126464 | tf_op jit(solution)/shard_map/dot_general | solution.py:121
  133.3 4.7 %all-to-all-start.2 = ((bf16[16,24,2048]{2,1,0:T(8,128)(2,1)}), bf16[16,24,2048]{2,1,0:T(8,128)(2,1)}, u32[]{:S(2)}, u32[]{:S(2)}) async-start(bf16[16,24,2048]{2,1,0:T(8,128)(2,1)} %bitcast.148), calls=%async_computation.2 | async-start | bytes 3145728 | tf_op jit(solution)/shard_map/all_to_all | solution.py:124
  138.1 0.0 copy-done.8
  138.1 0.3 fusion.137
  138.4 0.3 select_reduce_fusion.1
  138.8 20.0 %all-to-all-done.2 = bf16[16,24,2048]{2,1,0:T(8,128)(2,1)} async-done(((bf16[16,24,2048]{2,1,0:T(8,128)(2,1)}), bf16[16,24,2048]{2,1,0:T(8,128)(2,1)}, u32[]{:S(2)}, u32[]{:S(2)}) %all-to-all-start.2) | async-done | bytes 1572896 | tf_op jit(solution)/shard_map/all_to_all | solution.py:124
  158.8 6.7 %gather_fusion.1 = bf16[384,2048]{1,0:T(8,128)(2,1)} fusion(bf16[384,2048]{1,0:T(8,128)(2,1)} %bitcast.43, s32[1024]{0:T(1024)S(1)} %pad_clamp_fusion), kind=kCustom, calls=%fused_computation.1 | custom fusion | bytes 3147264 | tf_op jit(solution)/shard_map/gather | solution.py:132
  165.5 4.7 %reshape.154 = f32[192,2,2048]{2,1,0:T(2,128)} reshape(bf16[384,2048]{1,0:T(8,128)(2,1)} %gather_fusion.1) | data formatting | bytes 4718592 | tf_op jit(solution)/shard_map/convert_element_type | solution.py:134
  170.2 6.2 %fusion.138 = (f32[192,1,2048]{2,1,0:T(1,128)S(1)}, f32[192,1,2048]{2,1,0:T(1,128)S(1)}) fusion(f32[192,2,2048]{2,1,0:T(2,128)} %reshape.154), kind=kLoop, calls=%fused_computation.302 | loop fusion | bytes 6291456 | tf_op jit(solution)/shard_map/slice | solution.py:136
  176.4 2.6 %fusion.15 = bf16[192,2048]{1,0:T(8,128)(2,1)} fusion(f32[192,2048]{1,0:T(8,128)S(1)} %copy-done.2, f32[192,1,2048]{2,1,0:T(1,128)S(1)} %get-tuple-element.12, f32[192,1,2048]{2,1,0:T(1,128)S(1)} %get-tuple-element.11, f32[192]{0:T(256)S(1)} %multiply_divide_fusion, f32[192]{0:T(256)S(1)} %get-tuple-element.9), kind=kLoop, calls=%fused_computation.54 | loop fusion | flops 1966080 | bytes 5506560 | tf_op jit(solution)/shard_map/convert_element_type | solution.py:137
  (37 shorter events, 0.2 us)
Async XLA Ops:
  6.5 121.5 %copy-start = (bf16[1,512,2048]{2,1,0:T(8,128)(2,1)S(1)}, bf16[1,512,2048]{2,1,0:T(8,128)(2,1)}, u32[]{:S(2)}) copy-start(bf16[1,512,2048]{2,1,0:T(8,128)(2,1)} %param.29) | copy-start | bytes 6291460
  6.5 10.4 %copy-start.4 = (s32[3072]{0:T(1024)S(1)}, s32[3072]{0:T(1024)}, u32[]{:S(2)}) copy-start(s32[3072]{0:T(1024)} %param.17) | copy-start | bytes 36868
  6.5 10.3 %copy-start.9 = (bf16[31,128]{1,0:T(8,128)(2,1)S(1)}, bf16[31,128]{1,0:T(8,128)(2,1)}, u32[]{:S(2)}) copy-start(bf16[31,128]{1,0:T(8,128)(2,1)} %param.18) | copy-start | bytes 23812
  6.5 79.5 %all-gather.2.cloned.1.call-start = ((), (), s32[]{:S(2)}) async-start(), calls=%async_computation.3 | async-start | bytes 8912896 | tf_op jit(solution)/shard_map/all_gather | solution.py:18
  8.0 8.9 %collective-permute-start = (s32[30]{0:T(128)S(1)}, s32[30]{0:T(128)S(1)}, u32[]{:S(2)}, u32[]{:S(2)}) collective-permute-start(s32[30]{0:T(128)S(1)} %slice.297), channel_id=1, source_target_pairs={{0,16},{16,32},{32,48},{48,64},{64,80},{80,96},{96,112},{112,128},... | collective-permute-start | bytes 368 | tf_op jit(solution)/shard_map/ppermute | solution.py:12
  13.8 3.9 %collective-permute-start.1 = (bf16[30,128]{1,0:T(8,128)(2,1)S(1)}, bf16[30,128]{1,0:T(8,128)(2,1)S(1)}, u32[]{:S(2)}, u32[]{:S(2)}) collective-permute-start(bf16[30,128]{1,0:T(8,128)(2,1)S(1)} %slice.402), channel_id=1, source_target_pairs={{0,16},{16,32},{32,48},{48,64},{64,80},{80,96},{96,112},{112,128},... | collective-permute-start | bytes 23048 | tf_op jit(solution)/shard_map/ppermute | solution.py:12
  17.7 27.0 %copy-start.6 = (s32[192,2]{0,1:T(2,128)S(1)}, s32[192,2]{0,1:T(2,128)}, u32[]{:S(2)}) copy-start(s32[192,2]{0,1:T(2,128)} %param.26) | copy-start | bytes 4612
  34.2 51.8 %copy-start.11 = (f32[2048]{0:T(1024)S(1)}, f32[2048]{0:T(1024)}, u32[]{:S(2)}) copy-start(f32[2048]{0:T(1024)} %param.20) | copy-start | bytes 24580
  34.2 51.8 %copy-start.12 = (f32[2048]{0:T(1024)S(1)}, f32[2048]{0:T(1024)}, u32[]{:S(2)}) copy-start(f32[2048]{0:T(1024)} %param.19) | copy-start | bytes 24580
  34.2 40.5 %all-to-all-start = ((bf16[16,192,128]{2,1,0:T(8,128)(2,1)}), bf16[16,192,128]{2,1,0:T(8,128)(2,1)S(1)}, u32[]{:S(2)}, u32[]{:S(2)}) async-start(bf16[16,192,128]{2,1,0:T(8,128)(2,1)} %bitcast.147), calls=%async_computation | async-start | bytes 1572864 | tf_op jit(solution)/shard_map/all_to_all | solution.py:61
  75.3 17.7 %copy-start.7 = (f32[2048]{0:T(1024)S(1)}, f32[2048]{0:T(1024)}, u32[]{:S(2)}) copy-start(f32[2048]{0:T(1024)} %param.23) | copy-start | bytes 24580
  91.8 1.1 copy-start.1
  96.3 29.9 %copy-start.10 = (bf16[1,2048,512]{2,1,0:T(8,128)(2,1)S(1)}, bf16[1,2048,512]{2,1,0:T(8,128)(2,1)}, u32[]{:S(2)}) copy-start(bf16[1,2048,512]{2,1,0:T(8,128)(2,1)} %param.27) | copy-start | bytes 6291460
  125.0 1.2 copy-start.3
  133.3 4.7 %copy-start.8 = (bf16[2048,2]{0,1:T(2,128)(2,1)S(1)}, bf16[2048,2]{0,1:T(2,128)(2,1)}, u32[]{:S(2)}) copy-start(bf16[2048,2]{0,1:T(2,128)(2,1)} %param.24) | copy-start | bytes 24580
  133.3 5.1 %copy-start.5 = (bf16[2048,16]{0,1:T(8,128)(2,1)S(1)}, bf16[2048,16]{0,1:T(8,128)(2,1)}, u32[]{:S(2)}) copy-start(bf16[2048,16]{0,1:T(8,128)(2,1)} %param.25) | copy-start | bytes 196612
  133.3 25.5 %all-to-all-start.2 = ((bf16[16,24,2048]{2,1,0:T(8,128)(2,1)}), bf16[16,24,2048]{2,1,0:T(8,128)(2,1)}, u32[]{:S(2)}, u32[]{:S(2)}) async-start(bf16[16,24,2048]{2,1,0:T(8,128)(2,1)} %bitcast.148), calls=%async_computation.2 | async-start | bytes 3145728 | tf_op jit(solution)/shard_map/all_to_all | solution.py:124
  170.2 6.2 %copy-start.2 = (f32[192,2048]{1,0:T(8,128)S(1)}, f32[192,2048]{1,0:T(8,128)}, u32[]{:S(2)}) copy-start(f32[192,2048]{1,0:T(8,128)} %copy-done.1) | copy-start | bytes 4718596
Sparse Core Ops, SparseCore 0:
  9.2 76.8 all-gather.1
where the time goes:
time: 187 us; the launch traced here: 186 us
  waiting for transfers between devices  56.9 us (30%)
  blocking collectives  28.7 us (15%)
  local copies, waits for them, and re-layouts  27.6 us (15%)
  other arithmetic  23.2 us (12%)
  starting transfers between devices  22.2 us (12%)
  between operations  13.7 us (7%)
  matrix products  13.5 us (7%)
    all_to_all x1, blocking collectives, body(): lax.all_to_all(outgoing, 'sp', split_axis=0, concat_axis=0, tiled=True)  28.7 us
    all_to_all x1, waiting for transfers between devices, body(): lax.all_to_all(convolved, 'tp', split_axis=0, concat_axis=1, tiled=True)  25.1 us
    all_to_all x1, waiting for transfers between devices, body(): lax.all_to_all(expert_result.reshape(senders, slot_count, features), 'sp'...  20 us
    convert_element_type x1, other arithmetic, body(): convolved = summed.astype(jnp.bfloat16)  16.6 us
    all_gather x1, waiting for transfers between devices, project_rows(): lax.all_gather(proj_weight, 'tp', axis=0, tiled=True)  10.8 us
    all_to_all x1, starting transfers between devices, body(): lax.all_to_all(convolved, 'tp', split_axis=0, concat_axis=1, tiled=True)  10.4 us
    ppermute x2, starting transfers between devices, shifted(): return lax.ppermute(array, axis, pairs)  7.04 us
    gather x1, local copies, waits for them, and re-layouts, body(): returned.reshape(2 * row_count, normed.shape[1])[destination]  6.68 us
  transfers between devices with their start and end apart: 5, of which 4 were waited for; matrix products, arithmetic and copies ran while one was open for 14% of the time, Pallas kernels for 0%

commit v1 on v0

--- a/solution.py
+++ b/solution.py
@@ -1,15 +1,193 @@
+import functools
 import jax
 import jax.numpy as jnp
 from jax import lax
+from jax.experimental import pallas as pl
+from jax.experimental.pallas import tpu as pltpu
 from jax.sharding import PartitionSpec as P
 
 epsilon = 1e-06
-
-
-def shifted(array, axis, by):
-    count = lax.axis_size(axis)
-    pairs = [(i, i + by) for i in range(count) if 0 <= i + by < count]
-    return lax.ppermute(array, axis, pairs)
+MESH = pl.DeviceIdType.MESH
+F32 = jnp.float32
+BF16 = jnp.bfloat16
+
+
+def conv_kernel(
+    sp_size, tp_size, value_ref, gate_ref, ids_ref, taps_ref, raw_ref,
+    gated, reach, compact, outgoing, halo_ids, taps_wide,
+    send_sem, recv_sem, halo_send, halo_recv,
+):
+    s = lax.axis_index("sp")
+    t = lax.axis_index("tp")
+    planes = tp_size // 2
+    z, core = t // 2, t % 2
+    rows, width = value_ref.shape
+    block = rows // tp_size
+    taps = taps_ref.shape[0]
+    after, before = (s + 1) % sp_size, (s + sp_size - 1) % sp_size
+
+    barrier = pltpu.get_barrier_semaphore()
+
+    def greet(i, carry):
+        other = (t + 1 + i) % tp_size
+        pl.semaphore_signal(barrier, inc=1, device_id=(s, other), device_id_type=MESH)
+        return carry
+
+    lax.fori_loop(0, tp_size - 1, greet, 0)
+    pl.semaphore_signal(barrier, inc=1, device_id=(after, t), device_id_type=MESH)
+    pl.semaphore_signal(barrier, inc=1, device_id=(before, t), device_id_type=MESH)
+
+    def gate_rows(r, carry):
+        at = pl.multiple_of(r * 128, 128)
+        v = value_ref[pl.ds(at, 128), :].astype(F32)
+        g = gate_ref[pl.ds(at, 128), :].astype(F32)
+        gated[pl.ds(at + 32, 128), :] = (v * jax.nn.sigmoid(g)).astype(BF16).astype(F32)
+        return carry
+
+    chunks = rows // 128
+    gate_rows(chunks - 1, 0)
+    wide = taps_ref[...].astype(F32)
+    for k in range(taps):
+        taps_wide[k] = jnp.broadcast_to(wide[k : k + 1, :], (8, width))
+    pl.semaphore_wait(barrier, tp_size + 1)
+    halo = pltpu.make_async_remote_copy(
+        src_ref=gated.at[pl.ds(rows, 32)], dst_ref=gated.at[pl.ds(0, 32)],
+        send_sem=halo_send.at[0], recv_sem=halo_recv.at[0],
+        device_id=(after, t), device_id_type=MESH,
+    )
+    halo.start()
+    halo_id = pltpu.make_async_remote_copy(
+        src_ref=ids_ref.at[pl.ds(chunks - 8, 8)], dst_ref=halo_ids,
+        send_sem=halo_send.at[1], recv_sem=halo_recv.at[1],
+        device_id=(after, t), device_id_type=MESH,
+    )
+    halo_id.start()
+    lax.fori_loop(0, chunks - 1, gate_rows, 0)
+
+    ids = ids_ref[...]
+    lane = lax.broadcasted_iota(jnp.int32, (chunks, 128), 1)
+    row = lax.broadcasted_iota(jnp.int32, (chunks, 128), 0)
+    position = row * 128 + lane
+    began = jnp.zeros((chunks, 128), jnp.int32)
+    for d in range(1, 16):
+        count = jnp.sum(
+            jnp.sum((ids < d).astype(jnp.int32), axis=1, keepdims=True), axis=0, keepdims=True
+        )
+        began = jnp.where(ids == d, count, began)
+    halo_id.wait()
+    tail_lane = lax.broadcasted_iota(jnp.int32, (1, 128), 1)
+    shared = (halo_ids[7:8, :] == ids[0:1, 0:1]) & (tail_lane >= 128 - (taps - 1))
+    extra = jnp.sum(shared.astype(jnp.int32), axis=1, keepdims=True)
+    extra = extra * (s > 0).astype(jnp.int32)
+    distance = position - began + jnp.where(began == 0, extra, 0)
+    compact[...] = jnp.minimum(distance, taps).astype(F32)
+    eye = (
+        lax.broadcasted_iota(jnp.int32, (128, 128), 0)
+        == lax.broadcasted_iota(jnp.int32, (128, 128), 1)
+    ).astype(F32)
+    ones = jnp.ones((128, 128), BF16)
+
+    def widen(r, carry):
+        spread = (eye * compact[pl.ds(r, 1), :]).astype(BF16)
+        reach[pl.ds(pl.multiple_of(r * 128, 128), 128), :] = jnp.dot(
+            spread, ones, preferred_element_type=F32
+        )
+        return carry
+
+    lax.fori_loop(0, chunks, widen, 0)
+    halo.wait()
+
+    tile = 32
+
+    def conv_block(b, store):
+        def conv_tile(q, carry):
+            base = pl.multiple_of(b * block + q * tile, tile)
+            limit = reach[pl.ds(base, tile), :].reshape(tile // 8, 8, width)
+            total = jnp.zeros((tile // 8, 8, width), F32)
+            for k in range(taps):
+                j = taps - 1 - k
+                x = gated[pl.ds(base + (32 - j), tile), :].reshape(tile // 8, 8, width)
+                total = total + jnp.where(limit >= j, x * taps_wide[k][None], 0.0)
+            store(pl.multiple_of(q * tile, tile), total.reshape(tile, width).astype(BF16))
+            return carry
+
+        lax.fori_loop(0, block // tile, conv_tile, 0)
+
+    def target(i):
+        k = i // 2
+        size = planes // 2 - (k + 1) // 2
+        hop = (k % 2) * size + (1 - k % 2) * (planes - size)
+        return ((z + hop) % planes) * 2 + (core + 1 + i) % 2
+
+    def exchange(i):
+        to = target(i)
+        return pltpu.make_async_remote_copy(
+            src_ref=outgoing.at[to], dst_ref=raw_ref.at[t],
+            send_sem=send_sem.at[i], recv_sem=recv_sem.at[t],
+            device_id=(s, to), device_id_type=MESH,
+        )
+
+    def step(i, carry):
+        b = target(i)
+
+        def store(at, value):
+            outgoing[b, pl.ds(at, tile), :] = value
+
+        conv_block(b, store)
+
+        @pl.when(i > 0)
+        def _():
+            exchange(i - 1).start()
+
+        return carry
+
+    lax.fori_loop(0, tp_size - 1, step, 0)
+
+    def store_own(at, value):
+        raw_ref[t, pl.ds(at, tile), :] = value
+
+    conv_block(t, store_own)
+    exchange(tp_size - 2).start()
+
+    def finish(i, carry):
+        exchange(i).wait_send()
+        source = (t + 1 + i) % tp_size
+        pltpu.make_async_remote_copy(
+            src_ref=outgoing.at[source], dst_ref=raw_ref.at[source],
+            send_sem=send_sem.at[i], recv_sem=recv_sem.at[source],
+            device_id=(s, source), device_id_type=MESH,
+        ).wait_recv()
+        return carry
+
+    lax.fori_loop(0, tp_size - 1, finish, 0)
+
+
+def conv_exchange(mesh, conv_value, conv_gate, doc_ids, conv_kernel_taps):
+    sp_size, tp_size = mesh.shape["sp"], mesh.shape["tp"]
+    rows, width = conv_value.shape
+    block = rows // tp_size
+    taps = conv_kernel_taps.shape[0]
+    vmem = pl.BlockSpec(memory_space=pltpu.VMEM)
+    return pl.pallas_call(
+        functools.partial(conv_kernel, sp_size, tp_size),
+        out_shape=jax.ShapeDtypeStruct((tp_size, block, width), BF16),
+        in_specs=[vmem] * 4,
+        out_specs=vmem,
+        scratch_shapes=[
+            pltpu.VMEM((rows + 32, width), F32),
+            pltpu.VMEM((rows, width), F32),
+            pltpu.VMEM((rows // 128, 128), F32),
+            pltpu.VMEM((tp_size, block, width), BF16),
+            pltpu.VMEM((8, 128), jnp.int32),
+            pltpu.VMEM((taps, 8, width), F32),
+            pltpu.SemaphoreType.DMA((tp_size,)),
+            pltpu.SemaphoreType.DMA((tp_size,)),
+            pltpu.SemaphoreType.DMA((2,)),
+            pltpu.SemaphoreType.DMA((2,)),
+        ],
+        compiler_params=pltpu.CompilerParams(collective_id=0, has_side_effects=True),
+        cost_estimate=pl.CostEstimate(flops=30_000_000_000, bytes_accessed=4_000_000, transcendentals=0),
+    )(conv_value, conv_gate, doc_ids.reshape(rows // 128, 128), conv_kernel_taps)
 
 
 def project_rows(activated_rows, proj_weight):
@@ -21,6 +199,7 @@
 
 
 def body(
+    mesh,
     conv_value,
     conv_gate,
     doc_ids,
@@ -37,28 +216,8 @@
     expert_up_w,
     expert_down_w,
 ):
-    local_tokens, local_width = conv_value.shape
-    kernel_taps = conv_kernel.shape[0]
-    rim_width = kernel_taps - 1
-    gated_values = (
-        conv_value.astype(jnp.float32) * jax.nn.sigmoid(conv_gate.astype(jnp.float32))
-    ).astype(jnp.bfloat16)
-    rim_values, rim_ids = shifted(
-        (gated_values[local_tokens - rim_width :], doc_ids[local_tokens - rim_width :]), "sp", 1
-    )
-    padded = jnp.concatenate([rim_values, gated_values], axis=0)
-    padded_ids = jnp.concatenate([rim_ids, doc_ids], axis=0)
-    kernel = conv_kernel.astype(jnp.float32)
-    summed = jnp.zeros((local_tokens, local_width), jnp.float32)
-    for tap in range(kernel_taps):
-        same_doc = padded_ids[tap : tap + local_tokens] == doc_ids
-        summed = summed + jnp.where(
-            same_doc[:, None],
-            padded[tap : tap + local_tokens].astype(jnp.float32) * kernel[tap][None, :],
-            jnp.float32(0.0),
-        )
-    convolved = summed.astype(jnp.bfloat16)
-    raw_rows = lax.all_to_all(convolved, "tp", split_axis=0, concat_axis=1, tiled=True)
+    raw = conv_exchange(mesh, conv_value, conv_gate, doc_ids, conv_kernel)
+    raw_rows = raw.transpose(1, 0, 2).reshape(raw.shape[1], -1)
     raw_values = raw_rows.astype(jnp.float32)
     average = jnp.mean(raw_values, axis=1, keepdims=True)
     centered = raw_values - average
@@ -156,5 +315,5 @@
         P("sp", None, None),
     )
     return jax.shard_map(
-        body, mesh=mesh, in_specs=placed, out_specs=P(("sp", "tp"), None), check_vma=False
-    )
+        functools.partial(body, mesh), mesh=mesh, in_specs=placed, out_specs=P(("sp", "tp"), None), check_vma=False
+    )

time: 187 us -> 187 us (level)
  Pallas kernels: 0 us -> 48.8 us
  starting transfers between devices: 22.2 us -> 4.7 us
  other arithmetic: 23.2 us -> 7.44 us
  waiting for transfers between devices: 56.9 us -> 41.6 us
    pallas_call x0 -> x1, Pallas kernels: none -> 48.8 us  [conv_exchange(): pl.pallas_call(functools.partial(conv_kernel, sp_size, tp_size), out_shap...]
    all_to_all x1 -> x0, waiting for transfers between devices: 25.1 us -> none  [body(): lax.all_to_all(convolved, 'tp', split_axis=0, concat_axis=1, tiled=True)]
    convert_element_type x3 -> x0, other arithmetic: 18.4 us -> none  [the longest x1 16.6 us: body(): convolved = summed.astype(jnp.bfloat16)]
    all_to_all x1 -> x0, starting transfers between devices: 10.4 us -> none  [body(): lax.all_to_all(convolved, 'tp', split_axis=0, concat_axis=1, tiled=True)]
    all_gather x1, waiting for transfers between devices: 10.8 us -> 20.8 us  [project_rows(): lax.all_gather(proj_weight, 'tp', axis=0, tiled=True)]
    ppermute x2 -> x0, starting transfers between devices: 7.04 us -> none  [shifted(): return lax.ppermute(array, axis, pairs)]
  transfers between devices with their start and end apart: 5 -> 2, of which waited for: 4 -> 2; matrix products, arithmetic and copies ran while one was open for 14% -> 5% of each run, Pallas kernels for 0% -> 26%
where the time goes in v1:
time: 187 us; the launch traced here: 186 us
  Pallas kernels  48.8 us (26%)
  waiting for transfers between devices  41.6 us (22%)
  blocking collectives  28.8 us (15%)
  local copies, waits for them, and re-layouts  27.5 us (15%)
  between operations  13.6 us (7%)
  matrix products  13.5 us (7%)
  other arithmetic  7.44 us (4%)
  starting transfers between devices  4.7 us (3%)
    pallas_call x1, Pallas kernels, conv_exchange(): pl.pallas_call(functools.partial(conv_kernel, sp_size, tp_size), out_shap...  48.8 us
    all_to_all x1, blocking collectives, body(): lax.all_to_all(outgoing, 'sp', split_axis=0, concat_axis=0, tiled=True)  28.8 us
    all_gather x1, waiting for transfers between devices, project_rows(): lax.all_gather(proj_weight, 'tp', axis=0, tiled=True)  20.8 us
    all_to_all x1, waiting for transfers between devices, body(): lax.all_to_all(expert_result.reshape(senders, slot_count, features), 'sp'...  20 us
    gather x1, local copies, waits for them, and re-layouts, body(): returned.reshape(2 * row_count, normed.shape[1])[destination]  6.68 us
    slice x1, local copies, waits for them, and re-layouts, body(): picked[:, 0]  6.18 us
    dot_general x1, matrix products, project_rows(): jnp.dot(activated_rows, lax.all_gather(proj_weight, 'tp', axis=0, tiled=T...  5.7 us
    dot_general x1, matrix products, body(): jnp.dot(expert_hidden, expert_down_w[0], preferred_element_type=jnp.float32)  5.3 us
  transfers between devices with their start and end apart: 2, of which 2 were waited for; matrix products, arithmetic and copies ran while one was open for 5% of the time, Pallas kernels for 26%

profile of v1, /device:TPU:1, one launch (start us, length us, event | category | flops | bytes accessed | tf_op | source)
XLA Modules:
  0.0 185.9 jit_solution(14763283776863486912)
XLA Ops:
  6.5 0.0 copy-start
  6.5 0.0 all-gather.2.cloned.1.call-start
  6.5 0.7 all-gather.2.cloned.1.call-update
  7.3 0.8 copy.18
  8.1 0.1 eq.86
  8.2 0.1 eq.82
  8.4 0.9 reduce-window.6
  9.2 0.2 slice_reduce_fusion
  9.5 0.7 broadcast_multiply_fusion
  10.2 0.1 copy.17
  10.3 0.1 mul.115
  10.5 0.1 fusion.38
  10.6 2.9 %scatter_custom_fusion = s32[384]{0:T(512)S(1)} fusion(s32[384]{0:T(512)S(1)} %fusion.44, s32[384]{0:T(512)S(1)} %add_select_fusion, s32[]{:T(128)} %constant.48.clone.1), kind=kCustom, calls=%fused_computation.78 | custom fusion | bytes 1540 | tf_op jit(solution)/shard_map/scatter | solution.py:271
  13.5 48.8 %shard_map.145 = bf16[16,192,128]{2,1,0:T(8,128)(2,1)} custom-call(bf16[3072,128]{1,0:T(8,128)(2,1)} %value_ref.1, bf16[3072,128]{1,0:T(8,128)(2,1)} %gate_ref.1, s32[24,128]{1,0:T(8,128)} %bitcast.92, bf16[31,128]{1,0:T(8,128)(2,1)} %taps_ref.1), custom_call_target="tpu_custom_call" | custom-call | flops 30000001024 | bytes 4000000 | tf_op jit(solution)/shard_map/pallas_call | solution.py:171
  62.3 0.0 copy-start.3
  62.3 0.0 copy-start.10
  62.3 0.0 copy-start.11
  62.3 1.4 convert_reduce_fusion
  63.7 1.5 fusion.8
  65.2 0.0 copy-start.7
  65.3 20.8 %all-gather.2.cloned.1.call-done = bf16[2048,2048]{1,0:T(8,128)(2,1)} async-done(((bf16[128,2048]{1,0:T(8,128)(2,1)}), bf16[2048,2048]{1,0:T(8,128)(2,1)}) %all-gather.2.cloned.1.call-update) | async-done | bytes 8388624 | tf_op jit(solution)/shard_map/all_gather | solution.py:196
  86.1 0.0 copy-done.3
  86.1 0.0 copy-done.10
  86.1 0.0 copy-done.11
  86.1 5.7 %multiply_reduce_fusion = (f32[192]{0:T(256)S(1)}, f32[192,2048]{1,0:T(8,128)S(1)}) fusion(bf16[2048,2048]{1,0:T(8,128)(2,1)} %all-gather.2.cloned.1.call-done, f32[2048]{0:T(1024)S(1)} %copy-done.10, f32[2048]{0:T(1024)S(1)} %copy-done.11, f32[192]{0:T(256)S(1)} %add_rsqrt_fusion.1, f32[192]{0:T(256)S(1)} %broadcast_multiply_fusion.1, ...), kind=kOutput, calls=%fused_computation.29 | convolution fusion | flops 1616903936 | bytes 11553024 | tf_op jit(solution)/shard_map/dot_general | solution.py:194
  91.8 0.0 copy-start.1
  91.8 1.1 copy-done.1
  92.9 0.0 copy-done.7
  92.9 0.2 multiply_convert_fusion
  93.1 3.1 %gather_fusion = bf16[384,2048]{1,0:T(8,128)(2,1)} fusion(bf16[192,2048]{1,0:T(8,128)(2,1)S(1)} %multiply_convert_fusion, s32[1024]{0:T(1024)S(1)} %pad_clamp_fusion.1), kind=kCustom, calls=%fused_computation | custom fusion | bytes 3147264 | tf_op jit(solution)/shard_map/gather | solution.py:273
  96.3 28.8 %all_to_all.10 = bf16[16,24,2048]{2,1,0:T(8,128)(2,1)S(1)} all-to-all(bf16[16,24,2048]{2,1,0:T(8,128)(2,1)} %bitcast.84), channel_id=1, replica_groups=mesh['sp'=16,'tp'=16] {'sp'}, dimensions={0} | all-to-all | bytes 3145728 | tf_op jit(solution)/shard_map/all_to_all | solution.py:274
  125.0 1.2 copy-done.4
  126.2 0.0 copy-done.9
  126.2 1.9 fusion.5
  128.1 0.0 copy-done
  128.1 5.3 %convolution_convert_fusion = bf16[384,2048]{1,0:T(8,128)(2,1)} fusion(bf16[1,512,2048]{2,1,0:T(8,128)(2,1)S(1)} %copy-done, bf16[384,2048]{1,0:T(8,128)(2,1)} %bitcast.87, bf16[1,2048,512]{2,1,0:T(8,128)(2,1)} %param.28, f32[384,512]{1,0:T(8,128)} %fusion.5), kind=kOutput, calls=%fused_computation.3 | convolution fusion | flops 1612578816 | bytes 8126464 | tf_op jit(solution)/shard_map/dot_general | solution.py:280
  133.4 4.7 %all-to-all-start.1 = ((bf16[16,24,2048]{2,1,0:T(8,128)(2,1)}), bf16[16,24,2048]{2,1,0:T(8,128)(2,1)}, u32[]{:S(2)}, u32[]{:S(2)}) async-start(bf16[16,24,2048]{2,1,0:T(8,128)(2,1)} %bitcast.85), calls=%async_computation.1 | async-start | bytes 3145728 | tf_op jit(solution)/shard_map/all_to_all | solution.py:283
  138.1 0.0 copy-done.6
  138.1 0.0 copy-done.8
  138.1 0.3 fusion.49
  138.5 0.0 copy-done.5
  138.5 0.3 select_reduce_fusion.1
  138.8 20.0 %all-to-all-done.1 = bf16[16,24,2048]{2,1,0:T(8,128)(2,1)} async-done(((bf16[16,24,2048]{2,1,0:T(8,128)(2,1)}), bf16[16,24,2048]{2,1,0:T(8,128)(2,1)}, u32[]{:S(2)}, u32[]{:S(2)}) %all-to-all-start.1) | async-done | bytes 1572896 | tf_op jit(solution)/shard_map/all_to_all | solution.py:283
  158.9 6.7 %gather_fusion.1 = bf16[384,2048]{1,0:T(8,128)(2,1)} fusion(bf16[384,2048]{1,0:T(8,128)(2,1)} %bitcast.12, s32[1024]{0:T(1024)S(1)} %pad_clamp_fusion), kind=kCustom, calls=%fused_computation.1 | custom fusion | bytes 3147264 | tf_op jit(solution)/shard_map/gather | solution.py:291
  165.5 4.7 %reshape.126 = f32[192,2,2048]{2,1,0:T(2,128)} reshape(bf16[384,2048]{1,0:T(8,128)(2,1)} %gather_fusion.1) | data formatting | bytes 4718592 | tf_op jit(solution)/shard_map/convert_element_type | solution.py:293
  170.3 6.2 %fusion.50 = (f32[192,1,2048]{2,1,0:T(1,128)S(1)}, f32[192,1,2048]{2,1,0:T(1,128)S(1)}) fusion(f32[192,2,2048]{2,1,0:T(2,128)} %reshape.126), kind=kLoop, calls=%fused_computation.88 | loop fusion | bytes 6291456 | tf_op jit(solution)/shard_map/slice | solution.py:295
  176.5 0.0 copy-done.2
  176.5 2.6 %fusion.15 = bf16[192,2048]{1,0:T(8,128)(2,1)} fusion(f32[192,2048]{1,0:T(8,128)S(1)} %copy-done.2, f32[192,1,2048]{2,1,0:T(1,128)S(1)} %get-tuple-element.12, f32[192,1,2048]{2,1,0:T(1,128)S(1)} %get-tuple-element.11, f32[192]{0:T(256)S(1)} %multiply_divide_fusion, f32[192]{0:T(256)S(1)} %get-tuple-element.9), kind=kLoop, calls=%fused_computation.25 | loop fusion | flops 1966080 | bytes 5506560 | tf_op jit(solution)/shard_map/convert_element_type | solution.py:296
  (19 shorter events, 0.2 us)
Async XLA Ops:
  6.5 121.5 %copy-start = (bf16[1,512,2048]{2,1,0:T(8,128)(2,1)S(1)}, bf16[1,512,2048]{2,1,0:T(8,128)(2,1)}, u32[]{:S(2)}) copy-start(bf16[1,512,2048]{2,1,0:T(8,128)(2,1)} %param.29) | copy-start | bytes 6291460
  6.5 79.5 %all-gather.2.cloned.1.call-start = ((), (), s32[]{:S(2)}) async-start(), calls=%async_computation.2 | async-start | bytes 8912896 | tf_op jit(solution)/shard_map/all_gather | solution.py:196
  62.3 23.8 %copy-start.3 = (bf16[16,192,128]{2,1,0:T(8,128)(2,1)S(1)}, bf16[16,192,128]{2,1,0:T(8,128)(2,1)}, u32[]{:S(2)}) copy-start(bf16[16,192,128]{2,1,0:T(8,128)(2,1)} %shard_map.145) | copy-start | bytes 2359300
  62.3 23.8 %copy-start.10 = (f32[2048]{0:T(1024)S(1)}, f32[2048]{0:T(1024)}, u32[]{:S(2)}) copy-start(f32[2048]{0:T(1024)} %param.20) | copy-start | bytes 24580
  62.3 23.8 %copy-start.11 = (f32[2048]{0:T(1024)S(1)}, f32[2048]{0:T(1024)}, u32[]{:S(2)}) copy-start(f32[2048]{0:T(1024)} %param.19) | copy-start | bytes 24580
  65.2 27.7 %copy-start.7 = (f32[2048]{0:T(1024)S(1)}, f32[2048]{0:T(1024)}, u32[]{:S(2)}) copy-start(f32[2048]{0:T(1024)} %param.23) | copy-start | bytes 24580
  91.8 1.1 copy-start.1
  96.3 29.9 %copy-start.9 = (bf16[1,2048,512]{2,1,0:T(8,128)(2,1)S(1)}, bf16[1,2048,512]{2,1,0:T(8,128)(2,1)}, u32[]{:S(2)}) copy-start(bf16[1,2048,512]{2,1,0:T(8,128)(2,1)} %param.27) | copy-start | bytes 6291460
  125.0 1.2 copy-start.4
  133.4 4.7 %copy-start.6 = (s32[192,2]{0,1:T(2,128)S(1)}, s32[192,2]{0,1:T(2,128)}, u32[]{:S(2)}) copy-start(s32[192,2]{0,1:T(2,128)} %param.26) | copy-start | bytes 4612
  133.4 4.8 %copy-start.8 = (bf16[2048,2]{0,1:T(2,128)(2,1)S(1)}, bf16[2048,2]{0,1:T(2,128)(2,1)}, u32[]{:S(2)}) copy-start(bf16[2048,2]{0,1:T(2,128)(2,1)} %param.24) | copy-start | bytes 24580
  133.4 5.1 %copy-start.5 = (bf16[2048,16]{0,1:T(8,128)(2,1)S(1)}, bf16[2048,16]{0,1:T(8,128)(2,1)}, u32[]{:S(2)}) copy-start(bf16[2048,16]{0,1:T(8,128)(2,1)} %param.25) | copy-start | bytes 196612
  133.4 25.5 %all-to-all-start.1 = ((bf16[16,24,2048]{2,1,0:T(8,128)(2,1)}), bf16[16,24,2048]{2,1,0:T(8,128)(2,1)}, u32[]{:S(2)}, u32[]{:S(2)}) async-start(bf16[16,24,2048]{2,1,0:T(8,128)(2,1)} %bitcast.85), calls=%async_computation.1 | async-start | bytes 3145728 | tf_op jit(solution)/shard_map/all_to_all | solution.py:283
  170.3 6.2 %copy-start.2 = (f32[192,2048]{1,0:T(8,128)S(1)}, f32[192,2048]{1,0:T(8,128)}, u32[]{:S(2)}) copy-start(f32[192,2048]{1,0:T(8,128)} %copy-done.1) | copy-start | bytes 4718596
Sparse Core Ops, SparseCore 0:
  9.2 76.8 all-gather.1

commit v2 on v1

--- a/solution.py
+++ b/solution.py
@@ -190,11 +190,281 @@
     )(conv_value, conv_gate, doc_ids.reshape(rows // 128, 128), conv_kernel_taps)
 
 
-def project_rows(activated_rows, proj_weight):
-    return jnp.dot(
-        activated_rows,
-        lax.all_gather(proj_weight, "tp", axis=0, tiled=True),
-        preferred_element_type=jnp.float32,
+def route_kernel(
+    sp_size, raw_ref, weight_ref, residual_ref, gain_ref, bias_ref, moe_gain_ref,
+    group_router_ref, expert_router_ref, routing_ref, routed_ref,
+    gate_hbm, up_hbm, down_hbm, out_ref,
+    weight, gate_w, up_w, down_w, activated, hidden, normed, squares,
+    outgoing, arrived, results, returned,
+    weight_sem, expert_sem, send_sem, recv_sem, back_send, back_recv,
+):
+    s = lax.axis_index("sp")
+    t = lax.axis_index("tp")
+    side = 4
+    y, x = s // side, s % side
+    blocks, rows, width = raw_ref.shape
+    features = blocks * width
+    half = features // 2
+    slots = outgoing.shape[1] // 2
+
+    barrier = pltpu.get_barrier_semaphore()
+    for i in range(1, sp_size):
+        pl.semaphore_signal(
+            barrier, inc=1, device_id=((s + i) % sp_size, t), device_id_type=MESH
+        )
+
+    def fetch_weight(i):
+        return pltpu.make_async_copy(
+            weight_ref.at[pl.ds(2 * i, 2)], weight.at[pl.ds(2 * i, 2)], weight_sem.at[i]
+        )
+
+    pairs = weight.shape[0] // 2
+    for i in range(pairs):
+        fetch_weight(i).start()
+    fetch_experts = [
+        pltpu.make_async_copy(source.at[0], target, expert_sem.at[i])
+        for i, (source, target) in enumerate(
+            ((gate_hbm, gate_w), (up_hbm, up_w), (down_hbm, down_w))
+        )
+    ]
+    for copy in fetch_experts:
+        copy.start()
+
+    def activate(r, carry):
+        at = pl.multiple_of(r * 16, 16)
+        v = raw_ref[:, pl.ds(at, 16), :].astype(F32)
+        average = jnp.sum(jnp.sum(v, axis=0), axis=1, keepdims=True) * (1.0 / features)
+        centered = v - average[None]
+        variance = jnp.sum(jnp.sum(centered * centered, axis=0), axis=1, keepdims=True) * (
+            1.0 / features
+        )
+        scale = lax.rsqrt(variance + epsilon)
+        for b in range(blocks):
+            u = centered[b] * scale * gain_ref[b : b + 1, :] + bias_ref[b : b + 1, :]
+            activated[pl.ds(at, 16), b * width : (b + 1) * width] = jax.nn.silu(u).astype(BF16)
+        return carry
+
+    lax.fori_loop(0, rows // 16, activate, 0)
+
+    experts = expert_router_ref.shape[0]
+    e_lane = lax.broadcasted_iota(jnp.int32, (rows, experts), 1)
+    first, second = routing_ref[:, 0:1], routing_ref[:, 1:2]
+    pick_first, pick_second = first == e_lane, second == e_lane
+    named = (pick_first | pick_second).astype(F32)
+    lower = (
+        lax.broadcasted_iota(jnp.int32, (rows, rows), 0)
+        > lax.broadcasted_iota(jnp.int32, (rows, rows), 1)
+    ).astype(BF16)
+    earlier = jnp.dot(lower, named.astype(BF16), preferred_element_type=F32)
+    first_place = first * slots + jnp.sum(
+        jnp.where(pick_first, earlier, 0.0), axis=1, keepdims=True
+    ).astype(jnp.int32)
+    second_place = second * slots + jnp.sum(
+        jnp.where(pick_second, earlier, 0.0), axis=1, keepdims=True
+    ).astype(jnp.int32)
+
+    e_row = lax.broadcasted_iota(jnp.int32, (experts, rows), 0)
+    first_r, second_r = routed_ref[0:1, :], routed_ref[1:2, :]
+    pick_first_r, pick_second_r = first_r == e_row, second_r == e_row
+    named_r = (pick_first_r | pick_second_r).astype(F32)
+    upper = (
+        lax.broadcasted_iota(jnp.int32, (rows, rows), 0)
+        < lax.broadcasted_iota(jnp.int32, (rows, rows), 1)
+    ).astype(BF16)
+    earlier_r = jnp.dot(named_r.astype(BF16), upper, preferred_element_type=F32)
+    first_place_r = first_r * slots + jnp.sum(
+        jnp.where(pick_first_r, earlier_r, 0.0), axis=0, keepdims=True
+    ).astype(jnp.int32)
+    second_place_r = second_r * slots + jnp.sum(
+        jnp.where(pick_second_r, earlier_r, 0.0), axis=0, keepdims=True
+    ).astype(jnp.int32)
+
+    def expert_at(dy, dx):
+        return ((y + dy) % side) * side + (x + dx) % side
+
+    squares[...] = jnp.zeros_like(squares)
+
+    def project(i, carry):
+        fetch_weight(i).wait()
+        rhs = jnp.concatenate([weight[2 * i], weight[2 * i + 1]], axis=1)
+        total = jnp.dot(activated[...], rhs, preferred_element_type=F32)
+        columns = pl.ds(pl.multiple_of(i * 256, 256), 256)
+        state = (residual_ref[:, columns].astype(F32) + total).astype(BF16)
+        hidden[:, columns] = state
+        wide = state.astype(F32)
+        squared = wide * wide
+        squares[...] += squared[:, :128] + squared[:, 128:]
+        return carry
+
+    lax.fori_loop(0, pairs, project, 0)
+    moe_scale = lax.rsqrt(
+        jnp.sum(squares[...], axis=1, keepdims=True) * (1.0 / features) + epsilon
+    )
+    for f in range(blocks):
+        columns = slice(f * width, (f + 1) * width)
+        normed[:, columns] = (
+            hidden[:, columns].astype(F32) * moe_scale * moe_gain_ref[f : f + 1, :]
+        ).astype(BF16)
+
+    pl.semaphore_wait(barrier, sp_size - 1)
+    order = (2, 1, 3, 0)
+    columns_of = (2, 1, 3, 0)
+
+    def send(dy, dx):
+        i = dy * side + dx
+        return pltpu.make_async_remote_copy(
+            src_ref=outgoing.at[i], dst_ref=arrived.at[i],
+            send_sem=send_sem.at[i], recv_sem=recv_sem.at[i],
+            device_id=(expert_at(dy, dx), t), device_id_type=MESH,
+        )
+
+    def give_back(dy, dx):
+        i = dy * side + dx
+        return pltpu.make_async_remote_copy(
+            src_ref=results.at[i], dst_ref=returned.at[i],
+            send_sem=back_send.at[i], recv_sem=back_recv.at[i],
+            device_id=(expert_at(side - dy, side - dx), t), device_id_type=MESH,
+        )
+
+    def others(dy):
+        return [dx for dx in columns_of if dy or dx]
+
+    for dy in order:
+        slot = lax.broadcasted_iota(jnp.int32, (side, slots, rows), 1)
+        dx = lax.broadcasted_iota(jnp.int32, (side, slots, rows), 0)
+        key = ((((y + dy) % side) * side) + ((x + dx) & (side - 1))) * slots + slot
+        chosen = (
+            ((key == first_place_r[None]) | (key == second_place_r[None]))
+            .astype(F32)
+            .reshape(side * slots, rows)
+            .astype(BF16)
+        )
+        low = jnp.dot(chosen, normed[:, :half], preferred_element_type=F32)
+        high = jnp.dot(chosen, normed[:, half:], preferred_element_type=F32)
+        slab = jnp.concatenate(
+            [low.reshape(side, slots, half), high.reshape(side, slots, half)], axis=1
+        ).astype(BF16)
+        if dy == 0:
+            arrived[0] = slab[0]
+            outgoing[1:side] = slab[1:]
+        else:
+            outgoing[dy * side : (dy + 1) * side] = slab
+        for dx in others(dy):
+            send(dy, dx).start()
+
+    contract_last = (((1,), (1,)), ((), ()))
+    group_logits = lax.dot_general(
+        normed[...], group_router_ref[...], contract_last, preferred_element_type=F32
+    )
+    expert_logits = lax.dot_general(
+        normed[...], expert_router_ref[...], contract_last, preferred_element_type=F32
+    )
+    groups = group_router_ref.shape[0]
+    per_group = experts // groups
+    group_exp = jnp.exp(group_logits)
+    g_lane = lax.broadcasted_iota(jnp.int32, (rows, groups), 1)
+    in_group = (first >= g_lane * per_group) & (first < (g_lane + 1) * per_group)
+    group_prob = jnp.sum(jnp.where(in_group, group_exp, 0.0), axis=1, keepdims=True) / jnp.sum(
+        group_exp, axis=1, keepdims=True
+    )
+    first_exp = jnp.exp(jnp.sum(jnp.where(pick_first, expert_logits, 0.0), axis=1, keepdims=True))
+    second_exp = jnp.exp(
+        jnp.sum(jnp.where(pick_second, expert_logits, 0.0), axis=1, keepdims=True)
+    )
+    first_weight = group_prob * first_exp / (first_exp + second_exp)
+    second_weight = group_prob * second_exp / (first_exp + second_exp)
+
+    for copy in fetch_experts:
+        copy.wait()
+    for dy in order:
+        for dx in others(dy):
+            send(dy, dx).wait()
+        slab = arrived[dy * side : (dy + 1) * side].astype(F32)
+        low = slab[:, :slots].reshape(side * slots, half).astype(BF16)
+        high = slab[:, slots:].reshape(side * slots, half).astype(BF16)
+        gated = jnp.dot(low, gate_w[:half], preferred_element_type=F32) + jnp.dot(
+            high, gate_w[half:], preferred_element_type=F32
+        )
+        upped = jnp.dot(low, up_w[:half], preferred_element_type=F32) + jnp.dot(
+            high, up_w[half:], preferred_element_type=F32
+        )
+        inner = (jax.nn.silu(gated) * upped).astype(BF16)
+        low = jnp.dot(inner, down_w[:, :half], preferred_element_type=F32)
+        high = jnp.dot(inner, down_w[:, half:], preferred_element_type=F32)
+        slab = jnp.concatenate(
+            [low.reshape(side, slots, half), high.reshape(side, slots, half)], axis=1
+        ).astype(BF16)
+        if dy == 0:
+            returned[0] = slab[0]
+            results[1:side] = slab[1:]
+        else:
+            results[dy * side : (dy + 1) * side] = slab
+        for dx in others(dy):
+            give_back(dy, dx).start()
+
+    j = lax.broadcasted_iota(jnp.int32, (rows, sp_size * slots), 1)
+    i = (j * 2731) >> 16
+    key = (
+        ((y + (i >> 2)) & (side - 1)) * side + ((x + (i & (side - 1))) & (side - 1))
+    ) * slots + (j - i * slots)
+    first_hot = (key == first_place).astype(BF16)
+    second_hot = (key == second_place).astype(BF16)
+    for dy in order:
+        for dx in others(dy):
+            give_back(dy, dx).wait()
+
+    quarter = half // 4
+    for h in range(2):
+        for f in range(4):
+            part = returned[:, h * slots : (h + 1) * slots, f * quarter : (f + 1) * quarter]
+            part = part.astype(F32).reshape(sp_size * slots, quarter).astype(BF16)
+            columns = slice(h * half + f * quarter, h * half + (f + 1) * quarter)
+            mixed = first_weight * jnp.dot(
+                first_hot, part, preferred_element_type=F32
+            ) + second_weight * jnp.dot(second_hot, part, preferred_element_type=F32)
+            out_ref[:, columns] = (hidden[:, columns].astype(F32) + mixed).astype(BF16)
+
+
+def route(mesh, raw, weight, residual, gain, bias, moe_gain, group_router, expert_router, routing, gate_w, up_w, down_w):
+    sp_size = mesh.shape["sp"]
+    blocks, rows, width = raw.shape
+    features = blocks * width
+    slots = 2 * rows // sp_size
+    inner = gate_w.shape[2]
+    vmem = pl.BlockSpec(memory_space=pltpu.VMEM)
+    hbm = pl.BlockSpec(memory_space=pl.ANY)
+    slab = (sp_size, 2 * slots, features // 2)
+    return pl.pallas_call(
+        functools.partial(route_kernel, sp_size),
+        out_shape=jax.ShapeDtypeStruct((rows, features), BF16),
+        in_specs=[vmem, hbm, vmem, vmem, vmem, vmem, vmem, vmem, vmem, vmem, hbm, hbm, hbm],
+        out_specs=vmem,
+        scratch_shapes=[
+            pltpu.VMEM(weight.shape, BF16),
+            pltpu.VMEM((features, inner), BF16),
+            pltpu.VMEM((features, inner), BF16),
+            pltpu.VMEM((inner, features), BF16),
+            pltpu.VMEM((rows, features), BF16),
+            pltpu.VMEM((rows, features), BF16),
+            pltpu.VMEM((rows, features), BF16),
+            pltpu.VMEM((rows, 128), F32),
+            pltpu.VMEM(slab, BF16),
+            pltpu.VMEM(slab, BF16),
+            pltpu.VMEM(slab, BF16),
+            pltpu.VMEM(slab, BF16),
+            pltpu.SemaphoreType.DMA((weight.shape[0] // 2,)),
+            pltpu.SemaphoreType.DMA((3,)),
+            pltpu.SemaphoreType.DMA((sp_size,)),
+            pltpu.SemaphoreType.DMA((sp_size,)),
+            pltpu.SemaphoreType.DMA((sp_size,)),
+            pltpu.SemaphoreType.DMA((sp_size,)),
+        ],
+        compiler_params=pltpu.CompilerParams(collective_id=1, has_side_effects=True),
+        cost_estimate=pl.CostEstimate(flops=6_000_000_000, bytes_accessed=16_000_000, transcendentals=0),
+    )(
+        raw, weight, residual,
+        gain.reshape(blocks, width), bias.reshape(blocks, width), moe_gain.reshape(blocks, width),
+        group_router.T, expert_router.T, routing, routing.T, gate_w, up_w, down_w,
     )
 
 
@@ -216,84 +486,15 @@
     expert_up_w,
     expert_down_w,
 ):
+    part = proj_weight.shape[1] // mesh.shape["sp"]
+    own = lax.dynamic_slice_in_dim(proj_weight, lax.axis_index("sp") * part, part, axis=1)
+    weight = lax.all_gather(own, ("sp", "tp"), axis=0, tiled=True)
+    weight = weight.reshape(mesh.shape["sp"], proj_weight.shape[1], part)
     raw = conv_exchange(mesh, conv_value, conv_gate, doc_ids, conv_kernel)
-    raw_rows = raw.transpose(1, 0, 2).reshape(raw.shape[1], -1)
-    raw_values = raw_rows.astype(jnp.float32)
-    average = jnp.mean(raw_values, axis=1, keepdims=True)
-    centered = raw_values - average
-    variance = jnp.mean(centered * centered, axis=1, keepdims=True)
-    moved_rows = jax.nn.silu(
-        centered * lax.rsqrt(variance + epsilon) * norm_gain_conv + norm_bias_conv
-    ).astype(jnp.bfloat16)
-    projected = project_rows(moved_rows, proj_weight)
-    state_values = residual.astype(jnp.float32) + projected
-    hidden_state = state_values.astype(jnp.bfloat16)
-    state_values = hidden_state.astype(jnp.float32)
-    normed = (
-        state_values
-        * lax.rsqrt(jnp.mean(state_values * state_values, axis=1, keepdims=True) + epsilon)
-        * norm_gain_moe
-    ).astype(jnp.bfloat16)
-    group_logits = jnp.dot(normed, group_router, preferred_element_type=jnp.float32)
-    expert_logits = jnp.dot(normed, expert_router, preferred_element_type=jnp.float32)
-    group_total = group_router.shape[1]
-    expert_total = expert_router.shape[1]
-    per_group = expert_total // group_total
-    first_choice = routing[:, 0]
-    second_choice = routing[:, 1]
-    chosen_group = first_choice // per_group
-    group_exp = jnp.exp(group_logits)
-    group_match = chosen_group[:, None] == jnp.arange(group_total, dtype=jnp.int32)[None, :]
-    group_prob = jnp.sum(jnp.where(group_match, group_exp, jnp.float32(0.0)), axis=1) / jnp.sum(
-        group_exp, axis=1
-    )
-    expert_iota = jnp.arange(expert_total, dtype=jnp.int32)[None, :]
-    first_logit = jnp.sum(
-        jnp.where(first_choice[:, None] == expert_iota, expert_logits, jnp.float32(0.0)), axis=1
-    )
-    second_logit = jnp.sum(
-        jnp.where(second_choice[:, None] == expert_iota, expert_logits, jnp.float32(0.0)), axis=1
-    )
-    first_exp = jnp.exp(first_logit)
-    second_exp = jnp.exp(second_logit)
-    first_weight = group_prob * first_exp / (first_exp + second_exp)
-    second_weight = group_prob * second_exp / (first_exp + second_exp)
-    row_count = normed.shape[0]
-    capacity = 2 * row_count // expert_total
-    flat_experts = routing.reshape(-1)
-    indicator = (flat_experts[:, None] == expert_iota).astype(jnp.int32)
-    before = jnp.cumsum(indicator, axis=0) - indicator
-    position = jnp.sum(before * indicator, axis=1)
-    destination = flat_experts * capacity + position
-    source = (
-        jnp.zeros((2 * row_count,), jnp.int32)
-        .at[destination]
-        .set(jnp.arange(2 * row_count, dtype=jnp.int32) // 2)
-    )
-    outgoing = normed[source].reshape(expert_total, capacity, normed.shape[1])
-    arrived = lax.all_to_all(outgoing, "sp", split_axis=0, concat_axis=0, tiled=True)
-    senders, slot_count, features = arrived.shape
-    flattened = arrived.reshape(senders * slot_count, features)
-    gate_part = jnp.dot(flattened, expert_gate_w[0], preferred_element_type=jnp.float32)
-    up_part = jnp.dot(flattened, expert_up_w[0], preferred_element_type=jnp.float32)
-    expert_hidden = (jax.nn.silu(gate_part) * up_part).astype(jnp.bfloat16)
-    expert_result = jnp.dot(
-        expert_hidden, expert_down_w[0], preferred_element_type=jnp.float32
-    ).astype(jnp.bfloat16)
-    returned = lax.all_to_all(
-        expert_result.reshape(senders, slot_count, features),
-        "sp",
-        split_axis=0,
-        concat_axis=0,
-        tiled=True,
-    )
-    picked = (
-        returned.reshape(2 * row_count, normed.shape[1])[destination]
-        .reshape(row_count, 2, normed.shape[1])
-        .astype(jnp.float32)
-    )
-    mixture = first_weight[:, None] * picked[:, 0] + second_weight[:, None] * picked[:, 1]
-    return (state_values + mixture).astype(jnp.bfloat16)
+    return route(
+        mesh, raw, weight, residual, norm_gain_conv, norm_bias_conv, norm_gain_moe,
+        group_router, expert_router, routing, expert_gate_w, expert_up_w, expert_down_w,
+    )
 
 
 def solution(mesh):

time: 187 us -> 198 us (1.059)
  Pallas kernels: 48.8 us -> 95.3 us
  waiting for transfers between devices: 41.6 us -> 84.1 us
  blocking collectives: 28.8 us -> 0 us
  local copies, waits for them, and re-layouts: 27.5 us -> 5.18 us
  matrix products: 13.5 us -> 0 us
  other arithmetic: 7.44 us -> 0 us
  starting transfers between devices: 4.7 us -> 0.01 us
    all_gather x1, waiting for transfers between devices: 20.8 us -> 84.1 us  [body(): weight = lax.all_gather(own, ('sp', 'tp'), axis=0, tiled=True)]
    pallas_call x0 -> x1, Pallas kernels: none -> 54.7 us  [route(): pl.pallas_call(functools.partial(route_kernel, sp_size), out_shape=jax.Sh...]
    all_to_all x1 -> x0, blocking collectives: 28.8 us -> none  [body(): lax.all_to_all(outgoing, 'sp', split_axis=0, concat_axis=0, tiled=True)]
    all_to_all x1 -> x0, waiting for transfers between devices: 20 us -> none  [body(): lax.all_to_all(expert_result.reshape(senders, slot_count, features), 'sp'...]
    dot_general x5 -> x0, matrix products: 13.5 us -> none  [the longest x1 5.7 us: project_rows(): jnp.dot(activated_rows, lax.all_gather(proj_weight, 'tp', axis=0, tiled=T...]
    gather x2 -> x0, local copies, waits for them, and re-layouts: 9.81 us -> none  [the longest x1 6.68 us: body(): returned.reshape(2 * row_count, normed.shape[1])[destination]]
    pallas_call x1, Pallas kernels: 48.8 us -> 40.7 us  [conv_exchange(): pl.pallas_call(functools.partial(conv_kernel, sp_size, tp_size), out_shap...]
    slice x2 -> x0, local copies, waits for them, and re-layouts: 6.4 us -> none  [the longest x1 6.18 us: body(): picked[:, 0]]
  transfers between devices with their start and end apart: 2 -> 1, of which waited for: 2 -> 1; matrix products, arithmetic and copies ran while one was open for 5% -> 1% of each run, Pallas kernels for 26% -> 21%
where the time goes in v2:
time: 198 us
  Pallas kernels  95.3 us (48%)
  waiting for transfers between devices  84.1 us (42%)
  between operations  13.4 us (7%)
  local copies, waits for them, and re-layouts  5.18 us (3%)
    all_gather x1, waiting for transfers between devices, body(): weight = lax.all_gather(own, ('sp', 'tp'), axis=0, tiled=True)  84.1 us
    pallas_call x1, Pallas kernels, route(): pl.pallas_call(functools.partial(route_kernel, sp_size), out_shape=jax.Sh...  54.7 us
    pallas_call x1, Pallas kernels, conv_exchange(): pl.pallas_call(functools.partial(conv_kernel, sp_size, tp_size), out_shap...  40.7 us
    unnamed x4, local copies, waits for them, and re-layouts  4.57 us
  transfers between devices with their start and end apart: 1, of which 1 were waited for; matrix products, arithmetic and copies ran while one was open for 1% of the time, Pallas kernels for 21%

profile of v2, /device:TPU:1, one launch (start us, length us, event | category | flops | bytes accessed | tf_op | source)
XLA Modules:
  0.0 198.0 jit_solution(12820272314009048943)
XLA Ops:
  6.5 0.0 copy-start
  6.5 0.0 all-gather.2.cloned.1.call-start
  6.5 1.0 copy-done
  7.6 0.6 constant_dynamic-slice_fusion
  8.2 0.0 all-gather.2.cloned.1.call-update
  8.2 1.4 copy.16.routing_ref
  9.7 40.7 %shard_map.145.raw_ref = bf16[16,192,128]{2,1,0:T(8,128)(2,1)} custom-call(bf16[3072,128]{1,0:T(8,128)(2,1)} %value_ref.1, bf16[3072,128]{1,0:T(8,128)(2,1)} %gate_ref.1, s32[24,128]{1,0:T(8,128)} %bitcast.11, bf16[31,128]{1,0:T(8,128)(2,1)} %taps_ref.1), custom_call_target="tpu_custom_call" | custom-call | flops 30000001024 | bytes 4000000 | tf_op jit(solution)/shard_map/pallas_call | solution.py:171
  50.3 84.1 %all-gather.2.cloned.1.call-done = bf16[32768,128]{1,0:T(8,128)(2,1)} async-done(((bf16[128,128]{1,0:T(8,128)(2,1)}), bf16[32768,128]{1,0:T(8,128)(2,1)}) %all-gather.2.cloned.1.call-update) | async-done | bytes 8388624 | tf_op jit(solution)/shard_map/all_gather | solution.py:491
  134.4 54.7 %shard_map.146 = bf16[192,2048]{1,0:T(8,128)(2,1)} custom-call(bf16[16,192,128]{2,1,0:T(8,128)(2,1)} %shard_map.145.raw_ref, bf16[16,2048,128]{2,1,0:T(8,128)(2,1)} %bitcast.9, bf16[192,2048]{1,0:T(8,128)(2,1)} %residual_ref.1, f32[16,128]{1,0:T(8,128)} %bitcast.12, f32[16,128]{1,0:T(8,128)} %bitcast.13, f32[16,128]{1,0:T(8,128)} %bitcast.14, ...), custom_call_target="tpu_custom_call" | custom-call | flops 6000000000 | bytes 16000000 | tf_op jit(solution)/shard_map/pallas_call | solution.py:437
  189.1 2.1 %copy.18 = bf16[192,2048]{1,0:T(8,128)(2,1)} copy(bf16[192,2048]{1,0:T(8,128)(2,1)} %shard_map.146) | data formatting | bytes 1572864
Async XLA Ops:
  6.5 1.0 copy-start
  6.5 127.9 %all-gather.2.cloned.1.call-start = ((), (), s32[]{:S(2)}) async-start(), calls=%async_computation | async-start | bytes 8421376 | tf_op jit(solution)/shard_map/all_gather | solution.py:491
Sparse Core Ops, SparseCore 0:
  11.0 123.3 all-gather.1

commit v3 on v2

v3 whole, which is shorter than its diff:
```python
import functools
import jax
import jax.numpy as jnp
from jax import lax
from jax.experimental import pallas as pl
from jax.experimental.pallas import tpu as pltpu
from jax.sharding import PartitionSpec as P

epsilon = 1e-06
MESH = pl.DeviceIdType.MESH
F32 = jnp.float32
BF16 = jnp.bfloat16
SIDE = 4
PAIRS = (
    ((0, 0), (0, 1)), ((0, 3), (1, 0)), ((3, 0), (1, 1)), ((1, 3), (3, 1)),
    ((3, 3), (0, 2)), ((2, 0), (1, 2)), ((2, 1), (3, 2)), ((2, 3), (2, 2)),
)


def layer_kernel(
    sp_size, tp_size,
    value_hbm, gate_hbm, ids_ref, taps_ref, gain_ref, bias_ref, proj_hbm, residual_hbm,
    moe_gain_ref, group_router_ref, expert_router_ref, routed_ref, gate_hbm_w, up_hbm_w, down_hbm_w,
    out_ref,
    value_ref, gate_ref, residual_ref, gated, reach, compact, conv_out, raw, halo_ids, taps_wide,
    own_w, far_w, gate_w, up_w, down_w, activated, hidden, normed, squares,
    outgoing, arrived, results, returned,
    local_sem, expert_sem, conv_send, conv_recv, halo_send, halo_recv,
    z_send, z_recv, a_send, a_recv, b_send, b_recv, d_send, d_recv,
    send_sem, recv_sem, back_send, back_recv,
):
    s = lax.axis_index("sp")
    t = lax.axis_index("tp")
    y, x = s // SIDE, s % SIDE
    planes = tp_size // 2
    z, core = t // 2, t % 2
    rows, width = value_ref.shape
    block = rows // tp_size
    taps = taps_ref.shape[0]
    features = tp_size * width
    half = features // 2
    slots = outgoing.shape[1] // 2
    after, before = (s + 1) % sp_size, (s + sp_size - 1) % sp_size
    chunks = rows // 128

    barrier = pltpu.get_barrier_semaphore()

    def greet(i, carry):
        pl.semaphore_signal(
            barrier, inc=1, device_id=(s, (t + 1 + i) % tp_size), device_id_type=MESH
        )
        return carry

    def greet_plane(i, carry):
        pl.semaphore_signal(
            barrier, inc=1, device_id=((s + 1 + i) % sp_size, t), device_id_type=MESH
        )
        return carry

    lax.fori_loop(0, tp_size - 1, greet, 0)
    lax.fori_loop(0, sp_size - 1, greet_plane, 0)

    head = rows - 128
    local = [
        pltpu.make_async_copy(value_hbm.at[pl.ds(head, 128)], value_ref.at[pl.ds(head, 128)], local_sem.at[0]),
        pltpu.make_async_copy(gate_hbm.at[pl.ds(head, 128)], gate_ref.at[pl.ds(head, 128)], local_sem.at[1]),
        pltpu.make_async_copy(value_hbm.at[pl.ds(0, head)], value_ref.at[pl.ds(0, head)], local_sem.at[2]),
        pltpu.make_async_copy(gate_hbm.at[pl.ds(0, head)], gate_ref.at[pl.ds(0, head)], local_sem.at[3]),
        pltpu.make_async_copy(
            proj_hbm.at[:, pl.ds(pl.multiple_of(s * width, width), width)], own_w.at[0, 0, z], local_sem.at[4]
        ),
        pltpu.make_async_copy(residual_hbm, residual_ref, local_sem.at[5]),
    ]
    for copy in local:
        copy.start()
    fetch_experts = [
        pltpu.make_async_copy(source.at[0], target, expert_sem.at[i])
        for i, (source, target) in enumerate(
            ((gate_hbm_w, gate_w), (up_hbm_w, up_w), (down_hbm_w, down_w))
        )
    ]
    for copy in fetch_experts:
        copy.start()

    ids = ids_ref[...]
    lane = lax.broadcasted_iota(jnp.int32, (chunks, 128), 1)
    row = lax.broadcasted_iota(jnp.int32, (chunks, 128), 0)
    position = row * 128 + lane
    began = jnp.zeros((chunks, 128), jnp.int32)
    for d in range(1, 16):
        count = jnp.sum(
            jnp.sum((ids < d).astype(jnp.int32), axis=1, keepdims=True), axis=0, keepdims=True
        )
        began = jnp.where(ids == d, count, began)
    compact[...] = jnp.minimum(position - began, taps).astype(F32)
    wide = taps_ref[...].astype(F32)
    for k in range(taps):
        taps_wide[k] = jnp.broadcast_to(wide[k : k + 1, :], (8, width))
    eye = (
        lax.broadcasted_iota(jnp.int32, (128, 128), 0)
        == lax.broadcasted_iota(jnp.int32, (128, 128), 1)
    ).astype(F32)
    ones = jnp.ones((128, 128), BF16)

    def widen(r, carry):
        spread = (eye * compact[pl.ds(r, 1), :]).astype(BF16)
        reach[pl.ds(pl.multiple_of(r * 128, 128), 128), :] = jnp.dot(
            spread, ones, preferred_element_type=F32
        )
        return carry

    lax.fori_loop(0, chunks, widen, 0)

    def gate_rows(r, carry):
        at = pl.multiple_of(r * 128, 128)
        v = value_ref[pl.ds(at, 128), :].astype(F32)
        g = gate_ref[pl.ds(at, 128), :].astype(F32)
        gated[pl.ds(at + 32, 128), :] = (v * jax.nn.sigmoid(g)).astype(BF16).astype(F32)
        return carry

    local[0].wait()
    local[1].wait()
    gate_rows(chunks - 1, 0)
    local[4].wait()
    pl.semaphore_wait(barrier, tp_size + sp_size - 2)

    def z_copy(h):
        return pltpu.make_async_remote_copy(
            src_ref=own_w.at[0, 0, z], dst_ref=own_w.at[0, 0, z],
            send_sem=z_send.at[h], recv_sem=z_recv.at[z],
            device_id=(s, ((z + h) % planes) * 2 + core), device_id_type=MESH,
        )

    def z_arrival(h):
        source = (z + h) % planes
        return pltpu.make_async_remote_copy(
            src_ref=own_w.at[0, 0, source], dst_ref=own_w.at[0, 0, source],
            send_sem=z_send.at[h], recv_sem=z_recv.at[source],
            device_id=(s, source * 2 + core), device_id_type=MESH,
        )

    for h in (4, 3, 5, 2, 6, 1, 7):
        z_copy(h).start()
    halo_id = pltpu.make_async_remote_copy(
        src_ref=ids_ref.at[pl.ds(chunks - 8, 8)], dst_ref=halo_ids,
        send_sem=halo_send.at[1], recv_sem=halo_recv.at[1],
        device_id=(after, t), device_id_type=MESH,
    )
    halo_id.start()
    halo = pltpu.make_async_remote_copy(
        src_ref=gated.at[pl.ds(rows, 32)], dst_ref=gated.at[pl.ds(0, 32)],
        send_sem=halo_send.at[0], recv_sem=halo_recv.at[0],
        device_id=(after, t), device_id_type=MESH,
    )
    halo.start()
    local[2].wait()
    local[3].wait()
    lax.fori_loop(0, chunks - 1, gate_rows, 0)

    halo_id.wait()
    tail_lane = lax.broadcasted_iota(jnp.int32, (1, 128), 1)
    shared = (halo_ids[7:8, :] == ids[0:1, 0:1]) & (tail_lane >= 128 - (taps - 1))
    extra = jnp.sum(shared.astype(jnp.int32), axis=1, keepdims=True)
    extra = extra * (s > 0).astype(jnp.int32)
    distance = position[0:8] - began[0:8] + jnp.where(began[0:8] == 0, extra, 0)
    compact[0:8, :] = jnp.minimum(distance, taps).astype(F32)
    widen(0, 0)
    halo.wait()

    def along_q(d):
        return (1 - core) * (y * SIDE + (x + d) % SIDE) + core * (((y + d) % SIDE) * SIDE + x)

    def along_p(d):
        return core * (y * SIDE + (x + d) % SIDE) + (1 - core) * (((y + d) % SIDE) * SIDE + x)

    lower, upper = pl.ds(0, planes // 2), pl.ds(planes // 2, planes // 2)

    def a_copy(k):
        source, target, to = (
            (own_w.at[0, 0], own_w.at[0, 3], 1),
            (own_w.at[0, 0], own_w.at[0, 1], 3),
            (own_w.at[0, 3, lower], own_w.at[0, 2, lower], 1),
            (own_w.at[0, 1, upper], own_w.at[0, 2, upper], 3),
        )[k]
        return pltpu.make_async_remote_copy(
            src_ref=source, dst_ref=target, send_sem=a_send.at[k], recv_sem=a_recv.at[k],
            device_id=(along_q(to), t), device_id_type=MESH,
        )

    def b_copy(q, k):
        source, target, to = (
            (own_w.at[0, q], own_w.at[3, q], 1),
            (own_w.at[0, q], own_w.at[1, q], 3),
            (own_w.at[3, q, lower], own_w.at[2, q, lower], 1),
            (own_w.at[1, q, upper], own_w.at[2, q, upper], 3),
        )[k]
        return pltpu.make_async_remote_copy(
            src_ref=source, dst_ref=target, send_sem=b_send.at[q, k], recv_sem=b_recv.at[q, k],
            device_id=(along_p(to), t), device_id_type=MESH,
        )

    def d_copy(p, q):
        return pltpu.make_async_remote_copy(
            src_ref=own_w.at[p, q], dst_ref=far_w.at[p, q],
            send_sem=d_send.at[p, q], recv_sem=d_recv.at[p, q],
            device_id=(s, z * 2 + 1 - core), device_id_type=MESH,
        )

    def open_gather():
        for h in (1, 7, 2, 6, 3, 5, 4):
            z_arrival(h).wait_recv()
        a_copy(0).start()
        a_copy(1).start()
        b_copy(0, 0).start()
        b_copy(0, 1).start()
        d_copy(0, 0).start()

    tile = 32

    def conv_block(b, store):
        def conv_tile(q, carry):
            base = pl.multiple_of(b * block + q * tile, tile)
            limit = reach[pl.ds(base, tile), :].reshape(tile // 8, 8, width)
            total = jnp.zeros((tile // 8, 8, width), F32)
            for k in range(taps):
                j = taps - 1 - k
                v = gated[pl.ds(base + (32 - j), tile), :].reshape(tile // 8, 8, width)
                total = total + jnp.where(limit >= j, v * taps_wide[k][None], 0.0)
            store(pl.multiple_of(q * tile, tile), total.reshape(tile, width).astype(BF16))
            return carry

        lax.fori_loop(0, block // tile, conv_tile, 0)

    def target(i):
        k = i // 2
        size = planes // 2 - (k + 1) // 2
        hop = (k % 2) * size + (1 - k % 2) * (planes - size)
        return ((z + hop) % planes) * 2 + (core + 1 + i) % 2

    def exchange(i):
        to = target(i)
        return pltpu.make_async_remote_copy(
            src_ref=conv_out.at[to], dst_ref=raw.at[t],
            send_sem=conv_send.at[i], recv_sem=conv_recv.at[t],
            device_id=(s, to), device_id_type=MESH,
        )

    def step(i, carry):
        b = target(i)

        def store(at, value):
            conv_out[b, pl.ds(at, tile), :] = value

        conv_block(b, store)

        @pl.when(i > 0)
        def _():
            exchange(i - 1).start()

        @pl.when(i == 11)
        def _():
            open_gather()

        return carry

    lax.fori_loop(0, tp_size - 1, step, 0)

    def store_own(at, value):
        raw[t, pl.ds(at, tile), :] = value

    conv_block(t, store_own)
    exchange(tp_size - 2).start()

    for k in range(2):
        a_copy(k).wait_recv()
    for k in (2, 3):
        a_copy(k).start()
    for q in (3, 1):
        b_copy(q, 0).start()
        b_copy(q, 1).start()
        d_copy(0, q).start()

    experts = expert_router_ref.shape[0]
    e_row = lax.broadcasted_iota(jnp.int32, (experts, block), 0)
    first_r, second_r = routed_ref[0:1, :], routed_ref[1:2, :]
    pick_first_r, pick_second_r = first_r == e_row, second_r == e_row
    named_r = (pick_first_r | pick_second_r).astype(F32)
    token_r = lax.broadcasted_iota(jnp.int32, (block, block), 0)
    token_c = lax.broadcasted_iota(jnp.int32, (block, block), 1)
    earlier_r = jnp.dot(
        named_r.astype(BF16), (token_r < token_c).astype(BF16), preferred_element_type=F32
    )
    first_rank = jnp.sum(jnp.where(pick_first_r, earlier_r, 0.0), axis=0, keepdims=True)
    second_rank = jnp.sum(jnp.where(pick_second_r, earlier_r, 0.0), axis=0, keepdims=True)
    first_place_r = first_r * slots + first_rank.astype(jnp.int32)
    second_place_r = second_r * slots + second_rank.astype(jnp.int32)
    standing = jnp.concatenate(
        [
            first_r.astype(F32), second_r.astype(F32), first_rank, second_rank,
            jnp.zeros((4, block), F32),
        ],
        axis=0,
    ).astype(BF16)
    contract_last = (((1,), (1,)), ((), ()))
    turned = lax.dot_general(
        (token_r == token_c).astype(BF16), standing, contract_last, preferred_element_type=F32
    ).astype(jnp.int32)
    first, second = turned[:, 0:1], turned[:, 1:2]
    first_place = first * slots + turned[:, 2:3]
    second_place = second * slots + turned[:, 3:4]

    for k in (2, 3):
        a_copy(k).wait_recv()
    b_copy(2, 0).start()
    b_copy(2, 1).start()
    d_copy(0, 2).start()

    def relay(q):
        b_copy(q, 0).wait_recv()
        b_copy(q, 1).wait_recv()
        b_copy(q, 2).start()
        b_copy(q, 3).start()
        d_copy(3, q).start()
        d_copy(1, q).start()

    for q in (0, 3, 1):
        relay(q)

    def conv_arrival(i, carry):
        source = (t + 1 + i) % tp_size
        pltpu.make_async_remote_copy(
            src_ref=conv_out.at[source], dst_ref=raw.at[source],
            send_sem=conv_send.at[i], recv_sem=conv_recv.at[source],
            device_id=(s, source), device_id_type=MESH,
        ).wait_recv()
        return carry

    lax.fori_loop(0, tp_size - 1, conv_arrival, 0)

    def activate(r, carry):
        at = pl.multiple_of(r * 16, 16)
        v = raw[:, pl.ds(at, 16), :].astype(F32)
        average = jnp.sum(jnp.sum(v, axis=0), axis=1, keepdims=True) * (1.0 / features)
        centered = v - average[None]
        variance = jnp.sum(jnp.sum(centered * centered, axis=0), axis=1, keepdims=True) * (
            1.0 / features
        )
        scale = lax.rsqrt(variance + epsilon)
        for b in range(tp_size):
            u = centered[b] * scale * gain_ref[b : b + 1, :] + bias_ref[b : b + 1, :]
            activated[b % 2, pl.ds(at, 16), (b // 2) * width : (b // 2 + 1) * width] = (
                jax.nn.silu(u).astype(BF16)
            )
        return carry

    lax.fori_loop(0, block // 16, activate, 0)
    for q in (2,):
        relay(q)

    def expert_at(dy, dx):
        return ((y + dy) % SIDE) * SIDE + (x + dx) % SIDE

    squares[...] = jnp.zeros_like(squares)
    local[5].wait()

    def project(pair):
        def column(source, swap):
            parts = []
            for dy, dx in pair:
                i = dy * (1 - swap) + dx * swap
                k = dx * (1 - swap) + dy * swap
                parts.append(source[i, k].reshape(planes * width, width))
            return jnp.concatenate(parts, axis=1)

        total = jnp.dot(
            activated[core], column(own_w, core), preferred_element_type=F32
        ) + jnp.dot(activated[1 - core], column(far_w, 1 - core), preferred_element_type=F32)
        for n, (dy, dx) in enumerate(pair):
            columns = pl.ds(pl.multiple_of(expert_at(dy, dx) * width, width), width)
            state = (
                residual_ref[:, columns].astype(F32) + total[:, n * width : (n + 1) * width]
            ).astype(BF16)
            hidden[:, columns] = state
            wide_state = state.astype(F32)
            squares[...] += wide_state * wide_state

    near = (0, 1, 3)
    for p in near:
        for q in near:
            d_copy(p, q).wait_recv()
    for pair in PAIRS[:2]:
        project(pair)
    for q in (0, 3):
        b_copy(q, 2).wait_recv()
        b_copy(q, 3).wait_recv()
        d_copy(2, q).start()
    for pair in PAIRS[2:4]:
        project(pair)
    for q in (1, 2):
        b_copy(q, 2).wait_recv()
        b_copy(q, 3).wait_recv()
        d_copy(2, q).start()
    for p, q in ((0, 2), (1, 2), (3, 2), (2, 0), (2, 3), (2, 1), (2, 2)):
        d_copy(p, q).wait_recv()
    for pair in PAIRS[4:]:
        project(pair)

    moe_scale = lax.rsqrt(
        jnp.sum(squares[...], axis=1, keepdims=True) * (1.0 / features) + epsilon
    )
    for f in range(tp_size):
        columns = slice(f * width, (f + 1) * width)
        normed[:, columns] = (
            hidden[:, columns].astype(F32) * moe_scale * moe_gain_ref[f : f + 1, :]
        ).astype(BF16)

    order = (2, 1, 3, 0)
    columns_of = (2, 1, 3, 0)

    def send(dy, dx):
        i = dy * SIDE + dx
        return pltpu.make_async_remote_copy(
            src_ref=outgoing.at[i], dst_ref=arrived.at[i],
            send_sem=send_sem.at[i], recv_sem=recv_sem.at[i],
            device_id=(expert_at(dy, dx), t), device_id_type=MESH,
        )

    def give_back(dy, dx):
        i = dy * SIDE + dx
        return pltpu.make_async_remote_copy(
            src_ref=results.at[i], dst_ref=returned.at[i],
            send_sem=back_send.at[i], recv_sem=back_recv.at[i],
            device_id=(expert_at(SIDE - dy, SIDE - dx), t), device_id_type=MESH,
        )

    def others(dy):
        return [dx for dx in columns_of if dy or dx]

    for dy in order:
        slot = lax.broadcasted_iota(jnp.int32, (SIDE, slots, block), 1)
        dx = lax.broadcasted_iota(jnp.int32, (SIDE, slots, block), 0)
        key = ((((y + dy) % SIDE) * SIDE) + ((x + dx) & (SIDE - 1))) * slots + slot
        chosen = (
            ((key == first_place_r[None]) | (key == second_place_r[None]))
            .astype(F32)
            .reshape(SIDE * slots, block)
            .astype(BF16)
        )
        low = jnp.dot(chosen, normed[:, :half], preferred_element_type=F32)
        high = jnp.dot(chosen, normed[:, half:], preferred_element_type=F32)
        slab = jnp.concatenate(
            [low.reshape(SIDE, slots, half), high.reshape(SIDE, slots, half)], axis=1
        ).astype(BF16)
        if dy == 0:
            arrived[0] = slab[0]
            outgoing[1:SIDE] = slab[1:]
        else:
            outgoing[dy * SIDE : (dy + 1) * SIDE] = slab
        for dx in others(dy):
            send(dy, dx).start()

    group_logits = lax.dot_general(
        normed[...], group_router_ref[...], contract_last, preferred_element_type=F32
    )
    expert_logits = lax.dot_general(
        normed[...], expert_router_ref[...], contract_last, preferred_element_type=F32
    )
    e_lane = lax.broadcasted_iota(jnp.int32, (block, experts), 1)
    groups = group_router_ref.shape[0]
    per_group = experts // groups
    group_exp = jnp.exp(group_logits)
    g_lane = lax.broadcasted_iota(jnp.int32, (block, groups), 1)
    in_group = (first >= g_lane * per_group) & (first < (g_lane + 1) * per_group)
    group_prob = jnp.sum(jnp.where(in_group, group_exp, 0.0), axis=1, keepdims=True) / jnp.sum(
        group_exp, axis=1, keepdims=True
    )
    first_exp = jnp.exp(jnp.sum(jnp.where(first == e_lane, expert_logits, 0.0), axis=1, keepdims=True))
    second_exp = jnp.exp(
        jnp.sum(jnp.where(second == e_lane, expert_logits, 0.0), axis=1, keepdims=True)
    )
    first_weight = group_prob * first_exp / (first_exp + second_exp)
    second_weight = group_prob * second_exp / (first_exp + second_exp)

    for copy in fetch_experts:
        copy.wait()
    for dy in order:
        for dx in others(dy):
            send(dy, dx).wait()
        slab = arrived[dy * SIDE : (dy + 1) * SIDE].astype(F32)
        low = slab[:, :slots].reshape(SIDE * slots, half).astype(BF16)
        high = slab[:, slots:].reshape(SIDE * slots, half).astype(BF16)
        gated = jnp.dot(low, gate_w[:half], preferred_element_type=F32) + jnp.dot(
            high, gate_w[half:], preferred_element_type=F32
        )
        upped = jnp.dot(low, up_w[:half], preferred_element_type=F32) + jnp.dot(
            high, up_w[half:], preferred_element_type=F32
        )
        inner = (jax.nn.silu(gated) * upped).astype(BF16)
        low = jnp.dot(inner, down_w[:, :half], preferred_element_type=F32)
        high = jnp.dot(inner, down_w[:, half:], preferred_element_type=F32)
        slab = jnp.concatenate(
            [low.reshape(SIDE, slots, half), high.reshape(SIDE, slots, half)], axis=1
        ).astype(BF16)
        if dy == 0:
            returned[0] = slab[0]
            results[1:SIDE] = slab[1:]
        else:
            results[dy * SIDE : (dy + 1) * SIDE] = slab
        for dx in others(dy):
            give_back(dy, dx).start()

    j = lax.broadcasted_iota(jnp.int32, (block, sp_size * slots), 1)
    i = (j * 2731) >> 16
    key = (
        ((y + (i >> 2)) & (SIDE - 1)) * SIDE + ((x + (i & (SIDE - 1))) & (SIDE - 1))
    ) * slots + (j - i * slots)
    first_hot = (key == first_place).astype(BF16)
    second_hot = (key == second_place).astype(BF16)
    for dy in order:
        for dx in others(dy):
            give_back(dy, dx).wait()

    quarter = half // 4
    for h in range(2):
        for f in range(4):
            part = returned[:, h * slots : (h + 1) * slots, f * quarter : (f + 1) * quarter]
            part = part.astype(F32).reshape(sp_size * slots, quarter).astype(BF16)
            columns = slice(h * half + f * quarter, h * half + (f + 1) * quarter)
            mixed = first_weight * jnp.dot(
                first_hot, part, preferred_element_type=F32
            ) + second_weight * jnp.dot(second_hot, part, preferred_element_type=F32)
            out_ref[:, columns] = (hidden[:, columns].astype(F32) + mixed).astype(BF16)

    for i in range(tp_size - 1):
        exchange(i).wait_send()
    for h in range(1, planes):
        z_copy(h).wait_send()
    for k in range(4):
        a_copy(k).wait_send()
    for q in range(SIDE):
        for k in range(4):
            b_copy(q, k).wait_send()
    for p in range(SIDE):
        for q in range(SIDE):
            d_copy(p, q).wait_send()


def body(
    mesh, conv_value, conv_gate, doc_ids, conv_kernel, norm_gain_conv, norm_bias_conv,
    proj_weight, residual, norm_gain_moe, group_router, expert_router, routing,
    expert_gate_w, expert_up_w, expert_down_w,
):
    sp_size, tp_size = mesh.shape["sp"], mesh.shape["tp"]
    rows, width = conv_value.shape
    block = rows // tp_size
    features = tp_size * width
    taps = conv_kernel.shape[0]
    inner = expert_gate_w.shape[2]
    slots = 2 * block // sp_size
    planes = tp_size // 2
    vmem = pl.BlockSpec(memory_space=pltpu.VMEM)
    hbm = pl.BlockSpec(memory_space=pl.ANY)
    slab = (sp_size, 2 * slots, features // 2)
    dma = pltpu.SemaphoreType.DMA
    return pl.pallas_call(
        functools.partial(layer_kernel, sp_size, tp_size),
        out_shape=jax.ShapeDtypeStruct((block, features), BF16),
        in_specs=[hbm, hbm, vmem, vmem, vmem, vmem, hbm, hbm, vmem, vmem, vmem, vmem, hbm, hbm, hbm],
        out_specs=vmem,
        scratch_shapes=[
            pltpu.VMEM((rows, width), BF16),
            pltpu.VMEM((rows, width), BF16),
            pltpu.VMEM((block, features), BF16),
            pltpu.VMEM((rows + 32, width), F32),
            pltpu.VMEM((rows, width), F32),
            pltpu.VMEM((rows // 128, 128), F32),
            pltpu.VMEM((tp_size, block, width), BF16),
            pltpu.VMEM((tp_size, block, width), BF16),
            pltpu.VMEM((8, 128), jnp.int32),
            pltpu.VMEM((taps, 8, width), F32),
            pltpu.VMEM((SIDE, SIDE, planes, width, width), BF16),
            pltpu.VMEM((SIDE, SIDE, planes, width, width), BF16),
            pltpu.VMEM((features, inner), BF16),
            pltpu.VMEM((features, inner), BF16),
            pltpu.VMEM((inner, features), BF16),
            pltpu.VMEM((2, block, features // 2), BF16),
            pltpu.VMEM((block, features), BF16),
            pltpu.VMEM((block, features), BF16),
            pltpu.VMEM((block, 128), F32),
            pltpu.VMEM(slab, BF16),
            pltpu.VMEM(slab, BF16),
            pltpu.VMEM(slab, BF16),
            pltpu.VMEM(slab, BF16),
            dma((6,)), dma((3,)), dma((tp_size,)), dma((tp_size,)), dma((2,)), dma((2,)),
            dma((planes,)), dma((planes,)), dma((4,)), dma((4,)),
            dma((SIDE, 4)), dma((SIDE, 4)), dma((SIDE, SIDE)), dma((SIDE, SIDE)),
            dma((sp_size,)), dma((sp_size,)), dma((sp_size,)), dma((sp_size,)),
        ],
        compiler_params=pltpu.CompilerParams(collective_id=0, has_side_effects=True),
    )(
        conv_value, conv_gate, doc_ids.reshape(rows // 128, 128), conv_kernel,
        norm_gain_conv.reshape(tp_size, width), norm_bias_conv.reshape(tp_size, width),
        proj_weight, residual, norm_gain_moe.reshape(tp_size, width),
        group_router.T, expert_router.T, routing.T, expert_gate_w, expert_up_w, expert_down_w,
    )


def solution(mesh):
    placed = (
        P("sp", "tp"),
        P("sp", "tp"),
        P("sp"),
        P(None, "tp"),
        P(),
        P(),
        P("tp", None),
        P(("sp", "tp"), None),
        P(),
        P(),
        P(),
        P(("sp", "tp"), None),
        P("sp", None, None),
        P("sp", None, None),
        P("sp", None, None),
    )
    return jax.shard_map(
        functools.partial(body, mesh), mesh=mesh, in_specs=placed, out_specs=P(("sp", "tp"), None), check_vma=False
    )
```

time: 198 us -> 99.7 us (0.50)
  waiting for transfers between devices: 84.1 us -> 0 us
  between operations: 13.4 us -> 0.01 us
  local copies, waits for them, and re-layouts: 5.18 us -> 2.09 us
  Pallas kernels: 95.3 us -> 97.5 us
    all_gather x1 -> x0, waiting for transfers between devices: 84.1 us -> none  [body(): weight = lax.all_gather(own, ('sp', 'tp'), axis=0, tiled=True)]
    unnamed x4 -> x1, local copies, waits for them, and re-layouts: 4.57 us -> 2.09 us
    pallas_call x2 -> x1, Pallas kernels: 95.3 us -> 97.5 us  [body(): pl.pallas_call(functools.partial(layer_kernel, sp_size, tp_size), out_sha...]
  transfers between devices with their start and end apart: 1 -> 0, of which waited for: 1 -> 0; matrix products, arithmetic and copies ran while one was open for 1% -> 0% of each run, Pallas kernels for 21% -> 0%
where the time goes in v3:
time: 99.7 us; the launch traced here: 99.6 us
  Pallas kernels  97.5 us (98%)
  local copies, waits for them, and re-layouts  2.09 us (2%)
    pallas_call x1, Pallas kernels, body(): pl.pallas_call(functools.partial(layer_kernel, sp_size, tp_size), out_sha...  97.5 us
    unnamed x1, local copies, waits for them, and re-layouts  2.09 us

profile of v3, /device:TPU:1, one launch (start us, length us, event | category | flops | bytes accessed | tf_op | source)
XLA Modules:
  0.0 99.6 jit_solution(12588079010777446719)
XLA Ops:
  0.0 97.5 %shard_map.145 = bf16[192,2048]{1,0:T(8,128)(2,1)} custom-call(bf16[3072,128]{1,0:T(8,128)(2,1)} %value_hbm.1, bf16[3072,128]{1,0:T(8,128)(2,1)} %gate_hbm.1, s32[24,128]{1,0:T(8,128)} %bitcast.8, bf16[31,128]{1,0:T(8,128)(2,1)} %taps_ref.1, f32[16,128]{1,0:T(8,128)} %bitcast.9, f32[16,128]{1,0:T(8,128)} %bitcast.10, bf16[128,2048]{1,0:T(8,128)(2,1)} %proj_hbm.1, ...), custom_call_target="tpu_custom_call" | custom-call | tf_op jit(solution)/shard_map/pallas_call | solution.py:565
  97.5 2.1 %copy.17 = bf16[192,2048]{1,0:T(8,128)(2,1)} copy(bf16[192,2048]{1,0:T(8,128)(2,1)} %shard_map.145) | data formatting | bytes 1572864

commit v4 on v3

--- a/solution.py
+++ b/solution.py
@@ -11,6 +11,8 @@
 F32 = jnp.float32
 BF16 = jnp.bfloat16
 SIDE = 4
+HOPS = (0, 1, 7, 2, 6, 3, 5, 4)
+PIECES = ((1, 2), (3, 2), (5, 3))
 PAIRS = (
     ((0, 0), (0, 1)), ((0, 3), (1, 0)), ((3, 0), (1, 1)), ((1, 3), (3, 1)),
     ((3, 3), (0, 2)), ((2, 0), (1, 2)), ((2, 1), (3, 2)), ((2, 3), (2, 2)),
@@ -23,9 +25,9 @@
     moe_gain_ref, group_router_ref, expert_router_ref, routed_ref, gate_hbm_w, up_hbm_w, down_hbm_w,
     out_ref,
     value_ref, gate_ref, residual_ref, gated, reach, compact, conv_out, raw, halo_ids, taps_wide,
-    own_w, far_w, gate_w, up_w, down_w, activated, hidden, normed, squares,
+    first_w, own_w, far_w, gate_w, up_w, down_w, activated, hidden, normed, squares,
     outgoing, arrived, results, returned,
-    local_sem, expert_sem, conv_send, conv_recv, halo_send, halo_recv,
+    local_sem, rows_sem, expert_sem, conv_send, conv_recv, halo_send, halo_recv,
     z_send, z_recv, a_send, a_recv, b_send, b_recv, d_send, d_recv,
     send_sem, recv_sem, back_send, back_recv,
 ):
@@ -60,19 +62,37 @@
     lax.fori_loop(0, tp_size - 1, greet, 0)
     lax.fori_loop(0, sp_size - 1, greet_plane, 0)
 
+    def expert_at(dy, dx):
+        return ((y + dy) % SIDE) * SIDE + (x + dx) % SIDE
+
+    def block_at(p, q):
+        dy = (1 - core) * p + core * q
+        dx = (1 - core) * q + core * p
+        return expert_at(dy, dx)
+
     head = rows - 128
     local = [
         pltpu.make_async_copy(value_hbm.at[pl.ds(head, 128)], value_ref.at[pl.ds(head, 128)], local_sem.at[0]),
         pltpu.make_async_copy(gate_hbm.at[pl.ds(head, 128)], gate_ref.at[pl.ds(head, 128)], local_sem.at[1]),
-        pltpu.make_async_copy(value_hbm.at[pl.ds(0, head)], value_ref.at[pl.ds(0, head)], local_sem.at[2]),
-        pltpu.make_async_copy(gate_hbm.at[pl.ds(0, head)], gate_ref.at[pl.ds(0, head)], local_sem.at[3]),
         pltpu.make_async_copy(
-            proj_hbm.at[:, pl.ds(pl.multiple_of(s * width, width), width)], own_w.at[0, 0, z], local_sem.at[4]
+            proj_hbm.at[:, pl.ds(pl.multiple_of(s * width, width), width)], first_w, local_sem.at[2]
         ),
+        pltpu.make_async_copy(value_hbm.at[pl.ds(0, head)], value_ref.at[pl.ds(0, head)], local_sem.at[3]),
+        pltpu.make_async_copy(gate_hbm.at[pl.ds(0, head)], gate_ref.at[pl.ds(0, head)], local_sem.at[4]),
         pltpu.make_async_copy(residual_hbm, residual_ref, local_sem.at[5]),
     ]
     for copy in local:
         copy.start()
+
+    def own_rows(p, q):
+        return pltpu.make_async_copy(
+            proj_hbm.at[:, pl.ds(pl.multiple_of(block_at(p, q) * width, width), width)],
+            own_w.at[p, q, 0], rows_sem.at[p, q],
+        )
+
+    for p in range(SIDE):
+        for q in range(SIDE):
+            own_rows(p, q).start()
     fetch_experts = [
         pltpu.make_async_copy(source.at[0], target, expert_sem.at[i])
         for i, (source, target) in enumerate(
@@ -82,64 +102,56 @@
     for copy in fetch_experts:
         copy.start()
 
+    def gate_rows(at, size):
+        v = value_ref[pl.ds(at, size), :].astype(F32)
+        g = gate_ref[pl.ds(at, size), :].astype(F32)
+        gated[pl.ds(at + 32, size), :] = (v * jax.nn.sigmoid(g)).astype(BF16).astype(F32)
+
+    local[0].wait()
+    local[1].wait()
+    gate_rows(head, 128)
+
     ids = ids_ref[...]
     lane = lax.broadcasted_iota(jnp.int32, (chunks, 128), 1)
     row = lax.broadcasted_iota(jnp.int32, (chunks, 128), 0)
     position = row * 128 + lane
+    ones = jnp.ones((128, 128), BF16)
+    below = jnp.concatenate(
+        [jnp.sum((ids < d).astype(F32), axis=0, keepdims=True) for d in range(16)], axis=0
+    )
+    counts = jnp.dot(below.astype(BF16), ones, preferred_element_type=F32).astype(jnp.int32)
     began = jnp.zeros((chunks, 128), jnp.int32)
     for d in range(1, 16):
-        count = jnp.sum(
-            jnp.sum((ids < d).astype(jnp.int32), axis=1, keepdims=True), axis=0, keepdims=True
-        )
-        began = jnp.where(ids == d, count, began)
+        began = jnp.where(ids == d, counts[d : d + 1, :], began)
     compact[...] = jnp.minimum(position - began, taps).astype(F32)
-    wide = taps_ref[...].astype(F32)
-    for k in range(taps):
-        taps_wide[k] = jnp.broadcast_to(wide[k : k + 1, :], (8, width))
     eye = (
         lax.broadcasted_iota(jnp.int32, (128, 128), 0)
         == lax.broadcasted_iota(jnp.int32, (128, 128), 1)
     ).astype(F32)
-    ones = jnp.ones((128, 128), BF16)
-
-    def widen(r, carry):
-        spread = (eye * compact[pl.ds(r, 1), :]).astype(BF16)
-        reach[pl.ds(pl.multiple_of(r * 128, 128), 128), :] = jnp.dot(
-            spread, ones, preferred_element_type=F32
-        )
-        return carry
-
-    lax.fori_loop(0, chunks, widen, 0)
-
-    def gate_rows(r, carry):
-        at = pl.multiple_of(r * 128, 128)
-        v = value_ref[pl.ds(at, 128), :].astype(F32)
-        g = gate_ref[pl.ds(at, 128), :].astype(F32)
-        gated[pl.ds(at + 32, 128), :] = (v * jax.nn.sigmoid(g)).astype(BF16).astype(F32)
-        return carry
-
-    local[0].wait()
-    local[1].wait()
-    gate_rows(chunks - 1, 0)
-    local[4].wait()
-    pl.semaphore_wait(barrier, tp_size + sp_size - 2)
+
+    def widen(r, size):
+        spread = [(eye * compact[pl.ds(r + n, 1), :]).astype(BF16) for n in range(size)]
+        reach[pl.ds(pl.multiple_of(r * 128, 128), 128 * size), :] = jnp.dot(
+            jnp.concatenate(spread, axis=0), ones, preferred_element_type=F32
+        )
 
     def z_copy(h):
         return pltpu.make_async_remote_copy(
-            src_ref=own_w.at[0, 0, z], dst_ref=own_w.at[0, 0, z],
-            send_sem=z_send.at[h], recv_sem=z_recv.at[z],
+            src_ref=first_w, dst_ref=own_w.at[0, 0, HOPS.index(planes - h)],
+            send_sem=z_send.at[h], recv_sem=z_recv.at[planes - h],
             device_id=(s, ((z + h) % planes) * 2 + core), device_id_type=MESH,
         )
 
     def z_arrival(h):
-        source = (z + h) % planes
         return pltpu.make_async_remote_copy(
-            src_ref=own_w.at[0, 0, source], dst_ref=own_w.at[0, 0, source],
-            send_sem=z_send.at[h], recv_sem=z_recv.at[source],
-            device_id=(s, source * 2 + core), device_id_type=MESH,
-        )
-
-    for h in (4, 3, 5, 2, 6, 1, 7):
+            src_ref=first_w, dst_ref=own_w.at[0, 0, HOPS.index(h)],
+            send_sem=z_send.at[h], recv_sem=z_recv.at[h],
+            device_id=(s, ((z + h) % planes) * 2 + core), device_id_type=MESH,
+        )
+
+    local[2].wait()
+    pl.semaphore_wait(barrier, tp_size + sp_size - 2)
+    for h in HOPS[1:]:
         z_copy(h).start()
     halo_id = pltpu.make_async_remote_copy(
         src_ref=ids_ref.at[pl.ds(chunks - 8, 8)], dst_ref=halo_ids,
@@ -153,19 +165,37 @@
         device_id=(after, t), device_id_type=MESH,
     )
     halo.start()
-    local[2].wait()
+
+    def widen_step(r, carry):
+        widen(r * 8, 8)
+        return carry
+
+    lax.fori_loop(0, chunks // 8, widen_step, 0)
+    wide = taps_ref[...].astype(F32)
+    for k in range(taps):
+        taps_wide[k] = jnp.broadcast_to(wide[k : k + 1, :], (8, width))
     local[3].wait()
-    lax.fori_loop(0, chunks - 1, gate_rows, 0)
-
-    halo_id.wait()
-    tail_lane = lax.broadcasted_iota(jnp.int32, (1, 128), 1)
-    shared = (halo_ids[7:8, :] == ids[0:1, 0:1]) & (tail_lane >= 128 - (taps - 1))
-    extra = jnp.sum(shared.astype(jnp.int32), axis=1, keepdims=True)
-    extra = extra * (s > 0).astype(jnp.int32)
-    distance = position[0:8] - began[0:8] + jnp.where(began[0:8] == 0, extra, 0)
-    compact[0:8, :] = jnp.minimum(distance, taps).astype(F32)
-    widen(0, 0)
-    halo.wait()
+    local[4].wait()
+    gate_rows(head - 256, 256)
+
+    def gate_step(r, carry):
+        gate_rows(pl.multiple_of(r * 384, 128), 384)
+        return carry
+
+    lax.fori_loop(0, (head - 256) // 384, gate_step, 0)
+
+    def receive_halo():
+        halo_id.wait()
+        tail_lane = lax.broadcasted_iota(jnp.int32, (1, 128), 1)
+        shared = (halo_ids[7:8, :] == ids_ref[0:1, 0:1]) & (tail_lane >= 128 - (taps - 1))
+        extra = jnp.sum(shared.astype(F32), axis=1, keepdims=True)
+        extra = extra * (s > 0).astype(F32)
+        place = lax.broadcasted_iota(jnp.int32, (1, 128), 1).astype(F32)
+        near = compact[0:1, :]
+        joined = (near == place).astype(F32)
+        compact[0:1, :] = jnp.minimum(near + joined * extra, float(taps))
+        widen(0, 1)
+        halo.wait()
 
     def along_q(d):
         return (1 - core) * (y * SIDE + (x + d) % SIDE) + core * (((y + d) % SIDE) * SIDE + x)
@@ -173,31 +203,32 @@
     def along_p(d):
         return core * (y * SIDE + (x + d) % SIDE) + (1 - core) * (((y + d) % SIDE) * SIDE + x)
 
-    lower, upper = pl.ds(0, planes // 2), pl.ds(planes // 2, planes // 2)
-
-    def a_copy(k):
-        source, target, to = (
-            (own_w.at[0, 0], own_w.at[0, 3], 1),
-            (own_w.at[0, 0], own_w.at[0, 1], 3),
-            (own_w.at[0, 3, lower], own_w.at[0, 2, lower], 1),
-            (own_w.at[0, 1, upper], own_w.at[0, 2, upper], 3),
-        )[k]
+    rest, lower, upper = pl.ds(1, 7), pl.ds(1, 4), pl.ds(5, 3)
+
+    def remote(source, target, send, recv, to):
         return pltpu.make_async_remote_copy(
-            src_ref=source, dst_ref=target, send_sem=a_send.at[k], recv_sem=a_recv.at[k],
-            device_id=(along_q(to), t), device_id_type=MESH,
-        )
-
-    def b_copy(q, k):
-        source, target, to = (
-            (own_w.at[0, q], own_w.at[3, q], 1),
-            (own_w.at[0, q], own_w.at[1, q], 3),
-            (own_w.at[3, q, lower], own_w.at[2, q, lower], 1),
-            (own_w.at[1, q, upper], own_w.at[2, q, upper], 3),
-        )[k]
-        return pltpu.make_async_remote_copy(
-            src_ref=source, dst_ref=target, send_sem=b_send.at[q, k], recv_sem=b_recv.at[q, k],
-            device_id=(along_p(to), t), device_id_type=MESH,
-        )
+            src_ref=source, dst_ref=target, send_sem=send, recv_sem=recv,
+            device_id=(to, t), device_id_type=MESH,
+        )
+
+    def a_copy(k, n=0):
+        cut = pl.ds(*PIECES[n]) if k < 2 else (lower, upper)[k - 2]
+        origin, landing, to = ((0, 3, 1), (0, 1, 3), (3, 2, 1), (1, 2, 3))[k]
+        return remote(
+            own_w.at[0, origin, cut], own_w.at[0, landing, cut],
+            a_send.at[k, n], a_recv.at[k, n], along_q(to),
+        )
+
+    def b_copy(q, k, n=0):
+        cut = (pl.ds(*PIECES[n]) if q == 0 else rest) if k < 2 else (lower, upper)[k - 2]
+        origin, landing, to = ((0, 3, 1), (0, 1, 3), (3, 2, 1), (1, 2, 3))[k]
+        return remote(
+            own_w.at[origin, q, cut], own_w.at[landing, q, cut],
+            b_send.at[q, k, n], b_recv.at[q, k, n], along_p(to),
+        )
+
+    def pieces_of(q, k):
+        return len(PIECES) if k < 2 and q == 0 else 1
 
     def d_copy(p, q):
         return pltpu.make_async_remote_copy(
@@ -206,14 +237,16 @@
             device_id=(s, z * 2 + 1 - core), device_id_type=MESH,
         )
 
-    def open_gather():
-        for h in (1, 7, 2, 6, 3, 5, 4):
-            z_arrival(h).wait_recv()
-        a_copy(0).start()
-        a_copy(1).start()
-        b_copy(0, 0).start()
-        b_copy(0, 1).start()
-        d_copy(0, 0).start()
+    def open_gather(n):
+        for m in range(PIECES[n][0], PIECES[n][0] + PIECES[n][1]):
+            z_arrival(HOPS[m]).wait_recv()
+        a_copy(0, n).start()
+        a_copy(1, n).start()
+        b_copy(0, 0, n).start()
+        b_copy(0, 1, n).start()
+        if n == len(PIECES) - 1:
+            own_rows(0, 0).wait()
+            d_copy(0, 0).start()
 
     tile = 32
 
@@ -231,11 +264,23 @@
 
         lax.fori_loop(0, block // tile, conv_tile, 0)
 
-    def target(i):
+    def rank(i):
         k = i // 2
         size = planes // 2 - (k + 1) // 2
         hop = (k % 2) * size + (1 - k % 2) * (planes - size)
         return ((z + hop) % planes) * 2 + (core + 1 + i) % 2
+
+    early = rank(14)
+    met = sum((rank(i) == 0).astype(jnp.int32) for i in range(14))
+
+    def flag(truth):
+        return int(truth) if isinstance(truth, bool) else truth.astype(jnp.int32)
+
+    def target(i):
+        to = rank(i)
+        first = (to == 0).astype(jnp.int32) * flag(i < 14)
+        swap = flag(i == 14)
+        return (to + first * early) * (1 - swap * met)
 
     def exchange(i):
         to = target(i)
@@ -248,6 +293,10 @@
     def step(i, carry):
         b = target(i)
 
+        @pl.when(i == 14)
+        def _():
+            receive_halo()
+
         def store(at, value):
             conv_out[b, pl.ds(at, tile), :] = value
 
@@ -257,9 +306,11 @@
         def _():
             exchange(i - 1).start()
 
-        @pl.when(i == 11)
-        def _():
-            open_gather()
+        for n, at in enumerate((4, 8, 12)):
+
+            @pl.when(i == at)
+            def _(n=n):
+                open_gather(n)
 
         return carry
 
@@ -272,12 +323,14 @@
     exchange(tp_size - 2).start()
 
     for k in range(2):
-        a_copy(k).wait_recv()
+        for n in range(len(PIECES)):
+            a_copy(k, n).wait_recv()
     for k in (2, 3):
         a_copy(k).start()
     for q in (3, 1):
         b_copy(q, 0).start()
         b_copy(q, 1).start()
+        own_rows(0, q).wait()
         d_copy(0, q).start()
 
     experts = expert_router_ref.shape[0]
@@ -313,15 +366,24 @@
         a_copy(k).wait_recv()
     b_copy(2, 0).start()
     b_copy(2, 1).start()
+    own_rows(0, 2).wait()
     d_copy(0, 2).start()
 
     def relay(q):
-        b_copy(q, 0).wait_recv()
-        b_copy(q, 1).wait_recv()
+        for k in range(2):
+            for n in range(pieces_of(q, k)):
+                b_copy(q, k, n).wait_recv()
         b_copy(q, 2).start()
         b_copy(q, 3).start()
-        d_copy(3, q).start()
-        d_copy(1, q).start()
+        for p in (3, 1):
+            own_rows(p, q).wait()
+            d_copy(p, q).start()
+
+    def close(q):
+        b_copy(q, 2).wait_recv()
+        b_copy(q, 3).wait_recv()
+        own_rows(2, q).wait()
+        d_copy(2, q).start()
 
     for q in (0, 3, 1):
         relay(q)
@@ -346,19 +408,19 @@
             1.0 / features
         )
         scale = lax.rsqrt(variance + epsilon)
-        for b in range(tp_size):
-            u = centered[b] * scale * gain_ref[b : b + 1, :] + bias_ref[b : b + 1, :]
-            activated[b % 2, pl.ds(at, 16), (b // 2) * width : (b // 2 + 1) * width] = (
-                jax.nn.silu(u).astype(BF16)
-            )
+        for m in range(planes):
+            for side in range(2):
+                b = ((z + HOPS[m]) % planes) * 2 + side
+                u = raw[b, pl.ds(at, 16), :].astype(F32) - average
+                u = u * scale * gain_ref[pl.ds(b, 1), :] + bias_ref[pl.ds(b, 1), :]
+                activated[side, pl.ds(at, 16), m * width : (m + 1) * width] = (
+                    jax.nn.silu(u).astype(BF16)
+                )
         return carry
 
     lax.fori_loop(0, block // 16, activate, 0)
     for q in (2,):
         relay(q)
-
-    def expert_at(dy, dx):
-        return ((y + dy) % SIDE) * SIDE + (x + dx) % SIDE
 
     squares[...] = jnp.zeros_like(squares)
     local[5].wait()
@@ -391,15 +453,11 @@
     for pair in PAIRS[:2]:
         project(pair)
     for q in (0, 3):
-        b_copy(q, 2).wait_recv()
-        b_copy(q, 3).wait_recv()
-        d_copy(2, q).start()
+        close(q)
     for pair in PAIRS[2:4]:
         project(pair)
     for q in (1, 2):
-        b_copy(q, 2).wait_recv()
-        b_copy(q, 3).wait_recv()
-        d_copy(2, q).start()
+        close(q)
     for p, q in ((0, 2), (1, 2), (3, 2), (2, 0), (2, 3), (2, 1), (2, 2)):
         d_copy(p, q).wait_recv()
     for pair in PAIRS[4:]:
@@ -536,10 +594,12 @@
     for h in range(1, planes):
         z_copy(h).wait_send()
     for k in range(4):
-        a_copy(k).wait_send()
+        for n in range(pieces_of(0, k)):
+            a_copy(k, n).wait_send()
     for q in range(SIDE):
         for k in range(4):
-            b_copy(q, k).wait_send()
+            for n in range(pieces_of(q, k)):
+                b_copy(q, k, n).wait_send()
     for p in range(SIDE):
         for q in range(SIDE):
             d_copy(p, q).wait_send()
@@ -578,6 +638,7 @@
             pltpu.VMEM((tp_size, block, width), BF16),
             pltpu.VMEM((8, 128), jnp.int32),
             pltpu.VMEM((taps, 8, width), F32),
+            pltpu.VMEM((width, width), BF16),
             pltpu.VMEM((SIDE, SIDE, planes, width, width), BF16),
             pltpu.VMEM((SIDE, SIDE, planes, width, width), BF16),
             pltpu.VMEM((features, inner), BF16),
@@ -591,9 +652,9 @@
             pltpu.VMEM(slab, BF16),
             pltpu.VMEM(slab, BF16),
             pltpu.VMEM(slab, BF16),
-            dma((6,)), dma((3,)), dma((tp_size,)), dma((tp_size,)), dma((2,)), dma((2,)),
-            dma((planes,)), dma((planes,)), dma((4,)), dma((4,)),
-            dma((SIDE, 4)), dma((SIDE, 4)), dma((SIDE, SIDE)), dma((SIDE, SIDE)),
+            dma((6,)), dma((SIDE, SIDE)), dma((3,)), dma((tp_size,)), dma((tp_size,)), dma((2,)), dma((2,)),
+            dma((planes,)), dma((planes,)), dma((4, 3)), dma((4, 3)),
+            dma((SIDE, 4, 3)), dma((SIDE, 4, 3)), dma((SIDE, SIDE)), dma((SIDE, SIDE)),
             dma((sp_size,)), dma((sp_size,)), dma((sp_size,)), dma((sp_size,)),
         ],
         compiler_params=pltpu.CompilerParams(collective_id=0, has_side_effects=True),

time: 99.7 us -> 95.1 us (0.954)
  Pallas kernels: 97.5 us -> 92.8 us
    pallas_call x1, Pallas kernels: 97.5 us -> 92.8 us  [body(): pl.pallas_call(functools.partial(layer_kernel, sp_size, tp_size), out_sha...]
where the time goes in v4:
time: 95.1 us; the launch traced here: 94.9 us
  Pallas kernels  92.8 us (98%)
  local copies, waits for them, and re-layouts  2.09 us (2%)
    pallas_call x1, Pallas kernels, body(): pl.pallas_call(functools.partial(layer_kernel, sp_size, tp_size), out_sha...  92.8 us
    unnamed x1, local copies, waits for them, and re-layouts  2.09 us

profile of v4, /device:TPU:1, one launch (start us, length us, event | category | flops | bytes accessed | tf_op | source)
XLA Modules:
  0.0 94.9 jit_solution(7142588898288694975)
XLA Ops:
  0.0 92.8 %shard_map.145 = bf16[192,2048]{1,0:T(8,128)(2,1)} custom-call(bf16[3072,128]{1,0:T(8,128)(2,1)} %value_hbm.1, bf16[3072,128]{1,0:T(8,128)(2,1)} %gate_hbm.1, s32[24,128]{1,0:T(8,128)} %bitcast.8, bf16[31,128]{1,0:T(8,128)(2,1)} %taps_ref.1, f32[16,128]{1,0:T(8,128)} %bitcast.9, f32[16,128]{1,0:T(8,128)} %bitcast.10, bf16[128,2048]{1,0:T(8,128)(2,1)} %proj_hbm.1, ...), custom_call_target="tpu_custom_call" | custom-call | tf_op jit(solution)/shard_map/pallas_call | solution.py:625
  92.8 2.1 %copy.17 = bf16[192,2048]{1,0:T(8,128)(2,1)} copy(bf16[192,2048]{1,0:T(8,128)(2,1)} %shard_map.145) | data formatting | bytes 1572864

commit v5 on v4

--- a/solution.py
+++ b/solution.py
@@ -25,7 +25,7 @@
     moe_gain_ref, group_router_ref, expert_router_ref, routed_ref, gate_hbm_w, up_hbm_w, down_hbm_w,
     out_ref,
     value_ref, gate_ref, residual_ref, gated, reach, compact, conv_out, raw, halo_ids, taps_wide,
-    first_w, own_w, far_w, gate_w, up_w, down_w, activated, hidden, normed, squares,
+    first_w, own_w, far_w, gate_w, up_w, down_w, activated, hidden, normed, mixture, squares,
     outgoing, arrived, results, returned,
     local_sem, rows_sem, expert_sem, conv_send, conv_recv, halo_send, halo_recv,
     z_send, z_recv, a_send, a_recv, b_send, b_recv, d_send, d_recv,
@@ -400,8 +400,8 @@
     lax.fori_loop(0, tp_size - 1, conv_arrival, 0)
 
     def activate(r, carry):
-        at = pl.multiple_of(r * 16, 16)
-        v = raw[:, pl.ds(at, 16), :].astype(F32)
+        at = pl.multiple_of(r * 48, 48)
+        v = raw[:, pl.ds(at, 48), :].astype(F32)
         average = jnp.sum(jnp.sum(v, axis=0), axis=1, keepdims=True) * (1.0 / features)
         centered = v - average[None]
         variance = jnp.sum(jnp.sum(centered * centered, axis=0), axis=1, keepdims=True) * (
@@ -411,14 +411,14 @@
         for m in range(planes):
             for side in range(2):
                 b = ((z + HOPS[m]) % planes) * 2 + side
-                u = raw[b, pl.ds(at, 16), :].astype(F32) - average
+                u = raw[b, pl.ds(at, 48), :].astype(F32) - average
                 u = u * scale * gain_ref[pl.ds(b, 1), :] + bias_ref[pl.ds(b, 1), :]
-                activated[side, pl.ds(at, 16), m * width : (m + 1) * width] = (
+                activated[side, pl.ds(at, 48), m * width : (m + 1) * width] = (
                     jax.nn.silu(u).astype(BF16)
                 )
         return carry
 
-    lax.fori_loop(0, block // 16, activate, 0)
+    lax.fori_loop(0, block // 48, activate, 0)
     for q in (2,):
         relay(q)
 
@@ -472,7 +472,7 @@
             hidden[:, columns].astype(F32) * moe_scale * moe_gain_ref[f : f + 1, :]
         ).astype(BF16)
 
-    order = (2, 1, 3, 0)
+    order = (1, 3, 2, 0)
     columns_of = (2, 1, 3, 0)
 
     def send(dy, dx):
@@ -567,27 +567,37 @@
         for dx in others(dy):
             give_back(dy, dx).start()
 
-    j = lax.broadcasted_iota(jnp.int32, (block, sp_size * slots), 1)
-    i = (j * 2731) >> 16
-    key = (
-        ((y + (i >> 2)) & (SIDE - 1)) * SIDE + ((x + (i & (SIDE - 1))) & (SIDE - 1))
-    ) * slots + (j - i * slots)
-    first_hot = (key == first_place).astype(BF16)
-    second_hot = (key == second_place).astype(BF16)
-    for dy in order:
+    def hot(dy):
+        j = lax.broadcasted_iota(jnp.int32, (block, SIDE * slots), 1)
+        i = (j * 2731) >> 16
+        key = (((y + dy) % SIDE) * SIDE + ((x + i) & (SIDE - 1))) * slots + (j - i * slots)
+        return (key == first_place).astype(BF16), (key == second_place).astype(BF16)
+
+    hots = [hot(dy) for dy in order]
+    quarter = half // 4
+    for n, dy in enumerate(order):
         for dx in others(dy):
             give_back(dy, dx).wait()
-
-    quarter = half // 4
-    for h in range(2):
-        for f in range(4):
-            part = returned[:, h * slots : (h + 1) * slots, f * quarter : (f + 1) * quarter]
-            part = part.astype(F32).reshape(sp_size * slots, quarter).astype(BF16)
-            columns = slice(h * half + f * quarter, h * half + (f + 1) * quarter)
-            mixed = first_weight * jnp.dot(
-                first_hot, part, preferred_element_type=F32
-            ) + second_weight * jnp.dot(second_hot, part, preferred_element_type=F32)
-            out_ref[:, columns] = (hidden[:, columns].astype(F32) + mixed).astype(BF16)
+        first_part, second_part = hots[n]
+        for h in range(2):
+            for f in range(4):
+                part = returned[
+                    dy * SIDE : (dy + 1) * SIDE,
+                    h * slots : (h + 1) * slots, f * quarter : (f + 1) * quarter,
+                ]
+                part = part.astype(F32).reshape(SIDE * slots, quarter).astype(BF16)
+                columns = slice(h * half + f * quarter, h * half + (f + 1) * quarter)
+                mixed = first_weight * jnp.dot(
+                    first_part, part, preferred_element_type=F32
+                ) + second_weight * jnp.dot(second_part, part, preferred_element_type=F32)
+                if n == 0:
+                    mixture[:, columns] = mixed
+                elif n < len(order) - 1:
+                    mixture[:, columns] += mixed
+                else:
+                    out_ref[:, columns] = (
+                        hidden[:, columns].astype(F32) + (mixture[:, columns] + mixed)
+                    ).astype(BF16)
 
     for i in range(tp_size - 1):
         exchange(i).wait_send()
@@ -647,6 +657,7 @@
             pltpu.VMEM((2, block, features // 2), BF16),
             pltpu.VMEM((block, features), BF16),
             pltpu.VMEM((block, features), BF16),
+            pltpu.VMEM((block, features), F32),
             pltpu.VMEM((block, 128), F32),
             pltpu.VMEM(slab, BF16),
             pltpu.VMEM(slab, BF16),

time: 95.1 us -> 93.8 us (0.986)
  Pallas kernels: 92.8 us -> 90.9 us
    pallas_call x1, Pallas kernels: 92.8 us -> 90.9 us  [body(): pl.pallas_call(functools.partial(layer_kernel, sp_size, tp_size), out_sha...]
where the time goes in v5:
time: 93.8 us; the launch traced here: 93 us
  Pallas kernels  90.9 us (97%)
  local copies, waits for them, and re-layouts  2.09 us (2%)
    pallas_call x1, Pallas kernels, body(): pl.pallas_call(functools.partial(layer_kernel, sp_size, tp_size), out_sha...  90.9 us
    unnamed x1, local copies, waits for them, and re-layouts  2.09 us

profile of v5, /device:TPU:1, one launch (start us, length us, event | category | flops | bytes accessed | tf_op | source)
XLA Modules:
  0.0 93.0 jit_solution(1925464144659482349)
XLA Ops:
  0.0 90.9 %shard_map.145 = bf16[192,2048]{1,0:T(8,128)(2,1)} custom-call(bf16[3072,128]{1,0:T(8,128)(2,1)} %value_hbm.1, bf16[3072,128]{1,0:T(8,128)(2,1)} %gate_hbm.1, s32[24,128]{1,0:T(8,128)} %bitcast.8, bf16[31,128]{1,0:T(8,128)(2,1)} %taps_ref.1, f32[16,128]{1,0:T(8,128)} %bitcast.9, f32[16,128]{1,0:T(8,128)} %bitcast.10, bf16[128,2048]{1,0:T(8,128)(2,1)} %proj_hbm.1, ...), custom_call_target="tpu_custom_call" | custom-call | tf_op jit(solution)/shard_map/pallas_call | solution.py:635
  90.9 2.1 %copy.17 = bf16[192,2048]{1,0:T(8,128)(2,1)} copy(bf16[192,2048]{1,0:T(8,128)(2,1)} %shard_map.145) | data formatting | bytes 1572864
